TPU v7x, 32 devices: a whole 2x2x4 slice. The times are simulated.
32 devices in a mesh: grp: 2 (over y), sp: 4 (over z), tp: 4 (over x, core).
Axes of the slice: x: 2, y: 2, z: 4, core: 2. Of those that a mesh axis runs over, the one named last changes fastest.
Arguments:
- tokens_in: bfloat16 [3072, 4096], P(('grp', 'sp')), parts along dimension 0, may hold values from -6 to 6
- norm_gain: float32 [4096], replicated, may hold values from 0.1 to 1.9
- window_query: bfloat16 [4096, 1024], P('sp', 'tp'), may hold values from -0.09375 to 0.09375
- window_key: bfloat16 [4096, 512], P('sp', 'tp'), may hold values from -0.09375 to 0.09375
- window_value: bfloat16 [4096, 512], P('sp', 'tp'), may hold values from -0.09375 to 0.09375
- window_query_gain: float32 [64], replicated, may hold values from 0.6 to 16
- window_key_gain: float32 [64], replicated, may hold values from 0.6 to 16
- sink_logit: float32 [16], P('tp'), may hold values from 1 to 6
- dense_query: bfloat16 [4096, 1024], P('sp', 'tp'), may hold values from -0.09375 to 0.09375
- dense_key: bfloat16 [4096, 512], P('sp', 'tp'), may hold values from -0.09375 to 0.09375
- dense_value: bfloat16 [4096, 512], P('sp', 'tp'), may hold values from -0.09375 to 0.09375
- dense_query_gain: float32 [64], replicated, may hold values from 1 to 14
- dense_key_gain: float32 [64], replicated, may hold values from 1 to 14
- window_out: bfloat16 [1024, 4096], P('tp', 'sp'), may hold values from -1.5 to 1.5
- dense_out: bfloat16 [1024, 4096], P('tp', 'sp'), may hold values from -3 to 3
Outputs:
- mixed_out: bfloat16 [3072, 4096], P(('grp', 'sp', 'tp')), parts along dimension 0
There are 2 independent parts, one for each index of `grp`. A program takes and returns all parts, laid end to end along the dimension named above; an argument that names none is the same for every part. Nothing has to cross between parts.
All inputs are finite; a program needn't handle non-finite values.
Results may differ from a plain program's by a relative error of at most 0.03.
The roundings to bfloat16 on the way count: a program that leaves them out, or rounds other values in their place, can miss the bound.
Values may be sent and summed in bfloat16 or wider, within the bound.
A program may use at most 64 MiB of HBM per device.

v0:
```python
import functools

import jax
import jax.numpy as jnp
import numpy as np
from jax import lax
from jax.experimental import pallas as pl
from jax.experimental.pallas import tpu as pltpu
from jax.sharding import PartitionSpec as P

HD = 64
WINDOW = 128
GRID_W = 64


EPS = 1e-06
THETA = 10000.0


MESH = pl.DeviceIdType.MESH
HALVES = 2


class LineGather:
    def __init__(self, own, buf, z_recv, r_send, l_send, y_recv=None, y_send=None, axis=0):
        self.own, self.buf = own, buf
        self.z_recv, self.y_recv = z_recv, y_recv
        self.r_send, self.l_send, self.y_send = r_send, l_send, y_send
        self.n = lax.axis_size("sp")
        self.s = lax.axis_index("sp")
        self.shared = y_recv is not None
        self.g = lax.axis_index("grp") if self.shared else 0
        self.chunks = z_recv.shape[1]
        self.axis = axis
        extent = buf.shape[1 + axis]
        self.half = extent // HALVES if self.shared else extent
        self.size = self.half // self.chunks

    def rows(self, half, c):
        piece = pl.ds(pl.multiple_of(half * self.half + c * self.size, self.size), self.size)
        return (piece,) if self.axis == 0 else (slice(None), piece)

    def block(self, o, half, c):
        return self.buf.at[(o,) + self.rows(half, c)]

    def copy(self, src, o, c, sem, recv, target, half):
        return pltpu.make_async_remote_copy(
            src_ref=src,
            dst_ref=self.block(o, half, c),
            send_sem=sem.at[o, c],
            recv_sem=recv.at[o, c],
            device_id=target,
            device_id_type=MESH,
        )

    def right(self, src, o, c):
        return self.copy(src, o, c, self.r_send, self.z_recv, {"sp": lax.rem(self.s + 1, self.n)}, self.g)

    def left(self, src, o, c):
        return self.copy(
            src, o, c, self.l_send, self.z_recv, {"sp": lax.rem(self.s + self.n - 1, self.n)}, self.g
        )

    def twin(self, o, c, half):
        return self.copy(
            self.block(o, half, c), o, c, self.y_send, self.y_recv, {"grp": 1 - self.g}, half
        )

    def mine(self, c):
        if self.own is None:
            return self.block(self.s, self.g, c)
        return self.own.at[self.rows(self.g, c)]

    def start(self, first=0, last=None):
        for c in range(first, self.chunks if last is None else last):
            mine = self.mine(c)

            @pl.when(self.s + 1 < self.n)
            def _():
                self.right(mine, self.s, c).start()

            @pl.when(self.s > 0)
            def _():
                self.left(mine, self.s, c).start()

    def forward(self, d):
        for c in range(self.chunks):

            @pl.when(self.s - d >= 0)
            def _():
                o = self.s - d
                there = self.block(o, self.g, c)
                self.right(there, o, c).wait_recv()

                @pl.when(self.s + 1 < self.n)
                def _():
                    self.right(there, o, c).start()

                if self.shared:
                    self.twin(o, c, self.g).start()

            @pl.when(self.s + d < self.n)
            def _():
                o = self.s + d
                there = self.block(o, self.g, c)
                self.left(there, o, c).wait_recv()

                @pl.when(self.s > 0)
                def _():
                    self.left(there, o, c).start()

                if self.shared:
                    self.twin(o, c, self.g).start()

    def use(self, d, fn, near=None):
        for there, o in ((self.s - d >= 0, self.s - d), (self.s + d < self.n, self.s + d)):
            if near is not None:

                @pl.when(there)
                def _():
                    near(o)

        for there, o in ((self.s - d >= 0, self.s - d), (self.s + d < self.n, self.s + d)):

            @pl.when(there)
            def _():
                for c in range(self.chunks):
                    self.twin(o, c, 1 - self.g).wait_recv()
                fn(o)

    def run(self, fn, near=None, last=None):
        self.forward(1)
        self.rest(fn, near, last)

    def rest(self, fn, near=None, last=None):
        @pl.loop(2, self.n)
        def _(d):
            self.forward(d)
            self.use(d - 1, fn, near)

        if last is not None:
            last()
        self.use(self.n - 1, fn, near)

    def finish(self):
        @pl.loop(0, self.n)
        def _(o):
            for c in range(self.chunks):
                there = self.block(o, self.g, c)

                @pl.when((o <= self.s) & (self.s + 1 < self.n))
                def _():
                    self.right(there, o, c).wait_send()

                @pl.when((o >= self.s) & (self.s > 0))
                def _():
                    self.left(there, o, c).wait_send()

                if self.shared:

                    @pl.when(o != self.s)
                    def _():
                        self.twin(o, c, self.g).wait_send()


def greet():
    n, s, g = lax.axis_size("sp"), lax.axis_index("sp"), lax.axis_index("grp")
    n_tp, t = lax.axis_size("tp"), lax.axis_index("tp")
    barrier = pltpu.get_barrier_semaphore()
    pl.semaphore_signal(barrier, inc=1, device_id={"grp": 1 - g}, device_id_type=MESH)
    for j in range(1, n_tp):
        pl.semaphore_signal(barrier, inc=1, device_id={"tp": lax.rem(t + j, n_tp)}, device_id_type=MESH)

    @pl.when(s + 1 < n)
    def _():
        pl.semaphore_signal(barrier, inc=1, device_id={"sp": lax.rem(s + 1, n)}, device_id_type=MESH)

    @pl.when(s > 0)
    def _():
        pl.semaphore_signal(barrier, inc=1, device_id={"sp": lax.rem(s + n - 1, n)}, device_id_type=MESH)

    pl.semaphore_wait(barrier, n_tp + (s + 1 < n).astype(jnp.int32) + (s > 0).astype(jnp.int32))


LANES = 128


def by_half(low, high):
    lane = lax.broadcasted_iota(jnp.int32, low.shape, 1)
    return jnp.where(lane < HD, low, high)


def swap_pairs(values, reach):
    lane = lax.broadcasted_iota(jnp.int32, values.shape, 1)
    ahead = pltpu.roll(values, LANES - reach, 1)
    behind = pltpu.roll(values, reach, 1)
    return jnp.where(lax.rem(lane, 2 * reach) < reach, ahead, behind)


def head_tile(tile, kinds, gains_ref, tables_ref):
    square = tile * tile
    zero = jnp.zeros_like(square)
    low = jnp.sum(by_half(square, zero), axis=-1, keepdims=True)
    high = jnp.sum(by_half(zero, square), axis=-1, keepdims=True)
    mean = by_half(jnp.broadcast_to(low, tile.shape), jnp.broadcast_to(high, tile.shape)) * (1.0 / HD)
    scaled = tile * lax.rsqrt(mean + EPS)

    def one(kind):
        if kind is None:
            return tile
        gain, table, reach = kind
        normed = scaled * gains_ref[gain : gain + 1, :]
        return normed * tables_ref[2 * table] + swap_pairs(normed, reach) * tables_ref[2 * table + 1]

    if kinds[0] == kinds[1]:
        return one(kinds[0])
    return by_half(one(kinds[0]), one(kinds[1]))


def layer_kernel(
    sizes, x_ref, gain_ref, fixed_ref, g0, g1, g2, g3, sink_ref, *refs
):
    n_in = sizes[2]
    in_refs, out_refs = refs[:n_in], refs[n_in : n_in + 2]
    run_layer(sizes[:2], x_ref, gain_ref, fixed_ref, (g0, g1, g2, g3), sink_ref, in_refs, out_refs, *refs[n_in + 2 :])


def run_layer(
    sizes, x_ref, gain_ref, fixed_ref, head_gains, sink_ref, in_refs, out_refs, out_ref,
    small_ref, w_ref, wo_ref, tables_ref, load_sem, xn, proj, wbuf, wo_all, kvd, ext, qs, att, part, rs, halo_recv, halo_send, rs_recv, rs_send, *sems
):
    q_heads, kv_heads = sizes
    n, s = lax.axis_size("sp"), lax.axis_index("sp")
    n_tp, t = lax.axis_size("tp"), lax.axis_index("tp")
    depth = w_ref.shape[0]
    length = x_ref.shape[0]
    into = LineGather(w_ref, wbuf, *sems[:5])
    out = LineGather(wo_ref, wo_all, *sems[5:10], axis=1)
    keys = LineGather(None, kvd, *sems[10:])
    loads, at = [], 0
    for ref in in_refs:
        wide = ref.shape[1]
        loads.append(
            pltpu.make_async_copy(ref, w_ref.at[:, at : at + wide], load_sem.at[len(loads)])
        )
        at += wide
    at = 0
    for ref in out_refs:
        tall = ref.shape[0]
        loads.append(pltpu.make_async_copy(ref, wo_ref.at[at : at + tall], load_sem.at[len(loads)]))
        at += tall
    for load in loads:
        load.start()
    greet()
    for load in loads:
        load.wait()
    into.start()

    for k, ref in enumerate(head_gains):
        small_ref[k : k + 1, :] = jnp.concatenate([ref[...], ref[...]], axis=1)
    small_ref[4:8, :] = fixed_ref[...]
    step = 16

    @pl.loop(0, length // step)
    def _(i):
        rows = pl.ds(pl.multiple_of(i * step, step), step)
        values = x_ref[rows, :].astype(jnp.float32)
        mean = jnp.mean(values * values, axis=-1, keepdims=True)
        xn[rows, :] = (values * lax.rsqrt(mean + EPS) * gain_ref[...]).astype(jnp.bfloat16)

    def columns(o):
        return pl.ds(pl.multiple_of(o * depth, depth), depth)

    proj[...] = jnp.dot(xn[:, columns(s)], w_ref[...], preferred_element_type=jnp.float32)

    band = 64 if length % 64 == 0 else length

    @pl.loop(0, length // band)
    def _(i):
        rows = pl.ds(pl.multiple_of(i * band, band), band)
        shape = (band, LANES)
        place = lax.broadcasted_iota(jnp.int32, shape, 0) + (s * length + i * band)
        lane = lax.broadcasted_iota(jnp.int32, shape, 1)
        spot = jnp.where(lax.rem(lane, HD) < HD // 2, place // GRID_W, lax.rem(place, GRID_W))
        for k, where in enumerate((place, spot)):
            angles = where.astype(jnp.float32) * small_ref[4 + k : 5 + k, :]
            tables_ref[2 * k, rows, :] = jnp.cos(angles)
            tables_ref[2 * k + 1, rows, :] = jnp.sin(angles) * small_ref[6 + k : 7 + k, :]

    def add(o):
        proj[...] += jnp.dot(xn[:, columns(o)], wbuf[o], preferred_element_type=jnp.float32)

    into.run(add, last=lambda: out.start(0, 1))

    win_q, win_k, den_q, den_k = (0, 0, 32), (1, 0, 32), (2, 1, 16), (3, 1, 16)
    kinds = (
        [win_q] * q_heads + [den_q] * q_heads + [den_k] * kv_heads + [None] * kv_heads
        + [win_k] * kv_heads + [None] * kv_heads
    )
    q_tiles = 2 * q_heads * HD // LANES
    kv_tiles = 2 * kv_heads * HD // LANES

    def finished(i):
        return head_tile(
            proj[:, i * LANES : (i + 1) * LANES], kinds[2 * i : 2 * i + 2], small_ref, tables_ref
        )

    for i in range(kv_tiles):
        ext[WINDOW : WINDOW + length, i * LANES : (i + 1) * LANES] = finished(
            q_tiles + kv_tiles + i
        ).astype(jnp.bfloat16)
    for i in range(kv_tiles):
        kvd[s, :, i * LANES : (i + 1) * LANES] = finished(q_tiles + i).astype(jnp.bfloat16)

    def halo(side):
        source = pl.ds(length, WINDOW) if side == 0 else pl.ds(WINDOW, WINDOW)
        target = pl.ds(0, WINDOW) if side == 0 else pl.ds(WINDOW + length, WINDOW)
        peer = lax.rem(s + 1, n) if side == 0 else lax.rem(s + n - 1, n)
        return pltpu.make_async_remote_copy(
            src_ref=ext.at[source], dst_ref=ext.at[target], send_sem=halo_send.at[side],
            recv_sem=halo_recv.at[side], device_id={"sp": peer}, device_id_type=MESH,
        )

    has_right, has_left = s + 1 < n, s > 0

    @pl.when(has_right)
    def _():
        halo(0).start()

    @pl.when(has_left)
    def _():
        halo(1).start()

    keys.start()
    none = jnp.zeros((WINDOW, ext.shape[1]), jnp.bfloat16)

    @pl.when(jnp.logical_not(has_left))
    def _():
        ext[0:WINDOW, :] = none

    @pl.when(jnp.logical_not(has_right))
    def _():
        ext[WINDOW + length : WINDOW + length + WINDOW, :] = none

    group = q_heads // kv_heads

    def place(head):
        return head // 2, head % 2

    for i in range(q_tiles):
        tile = finished(i) * HD ** (-0.5)
        for b in range(2):
            head = 2 * i + b
            half = place((head % q_heads) // group)[1]
            moved = tile if half == b else pltpu.roll(tile, HD, 1)
            zero = jnp.zeros_like(moved)
            kept = by_half(moved, zero) if half == 0 else by_half(zero, moved)
            qs[head] = kept.astype(jnp.bfloat16)

    @pl.when(has_left)
    def _():
        halo(0).wait_recv()

    @pl.when(has_right)
    def _():
        halo(1).wait_recv()

    total_len = length * n

    def joined(results, heads):
        placed = []
        for b in range(2):
            half = place(kv_heads + heads[b] // group)[1]
            placed.append(results[b] if half == b else pltpu.roll(results[b], HD, 1))
        return by_half(placed[0], placed[1]).astype(jnp.bfloat16)

    def tile_of(head):
        return pl.ds(place(head)[0] * LANES, LANES)

    nt = (((1,), (1,)), ((), ()))

    def windowed(pair):
        @pl.loop(0, length // WINDOW)
        def _(b):
            base = pl.multiple_of(b * WINDOW, WINDOW)
            rows = pl.ds(base, WINDOW)
            near = pl.ds(base, 3 * WINDOW)
            shape = (WINDOW, 3 * WINDOW)
            at = lax.broadcasted_iota(jnp.int32, shape, 1) - WINDOW
            away = at - lax.broadcasted_iota(jnp.int32, shape, 0)
            pos = at + (s * length + base)
            valid = (away <= WINDOW) & (away >= -WINDOW) & (pos >= 0) & (pos < total_len)
            results = []
            for head in (2 * pair, 2 * pair + 1):
                key = ext[near, tile_of(head // group)]
                value = ext[near, tile_of(kv_heads + head // group)]
                scores = lax.dot_general(qs[head, rows, :], key, nt, preferred_element_type=jnp.float32)
                scores = jnp.where(valid, scores, -jnp.inf)
                floor = sink_ref[0, head]
                top = jnp.maximum(jnp.max(scores, axis=-1, keepdims=True), floor)
                expon = jnp.exp(scores - top)
                total = jnp.sum(expon, axis=-1, keepdims=True) + jnp.exp(floor - top)
                weights = (expon / total).astype(jnp.bfloat16)
                results.append(jnp.dot(weights, value, preferred_element_type=jnp.float32))
            att[rows, pair * LANES : (pair + 1) * LANES] = joined(results, (2 * pair, 2 * pair + 1))

    pairs = q_heads // 2
    keys.forward(1)
    windowed(0)

    @pl.loop(2, n)
    def _(d):
        keys.forward(d)

    out.start(1)
    for pair in range(1, pairs):
        windowed(pair)

    def dense(pair):
        @pl.loop(0, length // LANES)
        def _(b):
            rows = pl.ds(pl.multiple_of(b * LANES, LANES), LANES)
            results = []
            for head in (2 * pair, 2 * pair + 1):
                key = kvd[:, :, tile_of(head // group)].reshape(total_len, LANES)
                value = kvd[:, :, tile_of(kv_heads + head // group)].reshape(total_len, LANES)
                scores = lax.dot_general(
                    qs[q_heads + head, rows, :], key, nt, preferred_element_type=jnp.float32
                )
                top = jnp.max(scores, axis=-1, keepdims=True)
                expon = jnp.exp(scores - top)
                total = jnp.sum(expon, axis=-1, keepdims=True)
                summed = jnp.dot(
                    expon.astype(jnp.bfloat16), value, preferred_element_type=jnp.float32
                )
                results.append(summed / total)
            at = (pairs + pair) * LANES
            att[rows, at : at + LANES] = joined(results, (2 * pair, 2 * pair + 1))

    dense(0)
    out.forward(1)
    for pair in range(1, pairs):
        dense(pair)

    share = length // n_tp

    wide = wo_ref.shape[1]
    part_cols = wide // HALVES
    mine = lax.axis_index("grp")

    def span(h):
        return pl.ds(pl.multiple_of(h * part_cols, part_cols), part_cols)

    def exchange(o, h, j):
        peer = lax.rem(t + j, n_tp)
        return pltpu.make_async_remote_copy(
            src_ref=part.at[o, pl.ds(pl.multiple_of(peer * share, share), share), span(h)],
            dst_ref=rs.at[t, o, :, span(h)], send_sem=rs_send.at[j - 1, o, h],
            recv_sem=rs_recv.at[t, o, h], device_id={"tp": peer}, device_id_type=MESH,
        )

    def arrived(o, h, j):
        source = lax.rem(t + n_tp - j, n_tp)
        there = rs.at[source, o, :, span(h)]
        return pltpu.make_async_remote_copy(
            src_ref=there, dst_ref=there, send_sem=rs_send.at[j - 1, o, h],
            recv_sem=rs_recv.at[source, o, h], device_id={"tp": source}, device_id_type=MESH,
        )

    def emit(o, h, weight):
        part[o, :, span(h)] = jnp.dot(
            att[...], weight, preferred_element_type=jnp.float32
        ).astype(jnp.bfloat16)
        for j in range(1, n_tp):
            exchange(o, h, j).start()
        rs[t, o, :, span(h)] = part[o, pl.ds(pl.multiple_of(t * share, share), share), span(h)]

    def collect(o, h):
        for j in range(1, n_tp):
            arrived(o, h, j).wait_recv()
        total = rs[0, o, :, span(h)].astype(jnp.float32)
        for g in range(1, n_tp):
            total += rs[g, o, :, span(h)].astype(jnp.float32)
        columns_out = pl.ds(pl.multiple_of(o * wide + h * part_cols, part_cols), part_cols)
        out_ref[:, columns_out] = total.astype(jnp.bfloat16)

    for h in range(HALVES):
        emit(s, h, wo_ref[:, span(h)])
    out.rest(
        lambda o: emit(o, 1 - mine, wo_all[o, :, span(1 - mine)]),
        near=lambda o: emit(o, mine, wo_all[o, :, span(mine)]),
    )

    @pl.loop(0, n)
    def _(d):
        o = lax.rem(s + d, n)
        for h in range(HALVES):
            collect(o, h)

    @pl.loop(0, n)
    def _(o):
        for h in range(HALVES):
            for j in range(1, n_tp):
                exchange(o, h, j).wait_send()

    @pl.when(has_right)
    def _():
        halo(0).wait_send()

    @pl.when(has_left)
    def _():
        halo(1).wait_send()

    into.finish()
    out.finish()
    keys.finish()


def local(
    tokens_in,
    norm_gain,
    window_query,
    window_key,
    window_value,
    window_query_gain,
    window_key_gain,
    sink_logit,
    dense_query,
    dense_key,
    dense_value,
    dense_query_gain,
    dense_key_gain,
    window_out,
    dense_out,
):
    length, width = tokens_in.shape
    n, n_tp = lax.axis_size("sp"), lax.axis_size("tp")
    q_heads, kv_heads = window_query.shape[1] // HD, window_key.shape[1] // HD
    weights, held = [], []
    for weight in (window_query, dense_query, dense_key, dense_value, window_key, window_value):
        held.append(weight)
        if sum(w.shape[1] for w in held) % LANES == 0:
            weights.append(held[0] if len(held) == 1 else jnp.concatenate(held, axis=1))
            held = []
    depth, in_cols = window_query.shape[0], sum(w.shape[1] for w in weights)
    out_rows, out_cols = window_out.shape[0] + dense_out.shape[0], window_out.shape[1]

    lane = np.arange(LANES)
    fixed = np.stack(
        [THETA ** (-2.0 * (lane % (wide // 2)) / wide) for wide in (HD, HD // 2)]
        + [np.where(lane % wide < wide // 2, -1.0, 1.0) for wide in (HD, HD // 2)]
    ).astype(np.float32)
    gains = [g[None, :] for g in (window_query_gain, window_key_gain, dense_query_gain, dense_key_gain)]

    def gather(chunks):
        return [pltpu.SemaphoreType.DMA((n, chunks)) for _ in range(5)]

    in_chunks = 8 if n <= 4 else 1
    out_chunks = out_cols // HALVES // LANES if n <= 4 else 1
    kv_cols = 2 * kv_heads * HD
    vmem = pl.BlockSpec(memory_space=pltpu.VMEM)
    share = length // n_tp
    return pl.pallas_call(
        functools.partial(layer_kernel, (q_heads, kv_heads, len(weights))),
        out_shape=jax.ShapeDtypeStruct((share, width), jnp.bfloat16),
        in_specs=[vmem] * 7
        + [pl.BlockSpec(memory_space=pltpu.SMEM)]
        + [pl.BlockSpec(memory_space=pl.ANY)] * (len(weights) + 2),
        out_specs=vmem,
        scratch_shapes=[
            pltpu.VMEM((8, LANES), jnp.float32),
            pltpu.VMEM((depth, in_cols), jnp.bfloat16),
            pltpu.VMEM((out_rows, out_cols), jnp.bfloat16),
            pltpu.VMEM((4, length, LANES), jnp.float32),
            pltpu.SemaphoreType.DMA((len(weights) + 2,)),
            pltpu.VMEM((length, width), jnp.bfloat16),
            pltpu.VMEM((length, in_cols), jnp.float32),
            pltpu.VMEM((n, depth, in_cols), jnp.bfloat16),
            pltpu.VMEM((n, out_rows, out_cols), jnp.bfloat16),
            pltpu.VMEM((n, length, kv_cols), jnp.bfloat16),
            pltpu.VMEM((length + 2 * WINDOW, kv_cols), jnp.bfloat16),
            pltpu.VMEM((2 * q_heads, length, LANES), jnp.bfloat16),
            pltpu.VMEM((length, out_rows), jnp.bfloat16),
            pltpu.VMEM((n, length, out_cols), jnp.bfloat16),
            pltpu.VMEM((n_tp, n, share, out_cols), jnp.bfloat16),
            pltpu.SemaphoreType.DMA((2,)),
            pltpu.SemaphoreType.DMA((2,)),
            pltpu.SemaphoreType.DMA((n_tp, n, HALVES)),
            pltpu.SemaphoreType.DMA((n_tp - 1, n, HALVES)),
        ]
        + gather(in_chunks)
        + gather(out_chunks)
        + [pltpu.SemaphoreType.DMA((n, 2 if n <= 4 else 1)) for _ in range(3)],
        compiler_params=pltpu.CompilerParams(
            collective_id=0, has_side_effects=True, vmem_limit_bytes=62 * 1024 * 1024
        ),
    )(tokens_in, norm_gain[None, :], fixed, *gains, sink_logit[None, :], *weights, window_out, dense_out)


def solution(mesh):
    return jax.shard_map(
        local,
        mesh=mesh,
        in_specs=(
            P(("grp", "sp"), None),
            P(),
            P("sp", "tp"),
            P("sp", "tp"),
            P("sp", "tp"),
            P(),
            P(),
            P("tp"),
            P("sp", "tp"),
            P("sp", "tp"),
            P("sp", "tp"),
            P(),
            P(),
            P("tp", "sp"),
            P("tp", "sp"),
        ),
        out_specs=P(("grp", "sp", "tp"), None),
        check_vma=False,
    )
```

profile of v0, /device:TPU:0, one launch (start us, length us, event | category | flops | bytes accessed | tf_op | source)
XLA Modules:
  0.0 154.9 jit_solution(14210864217597900097)
XLA Ops:
  0.0 152.8 %shard_map.154 = bf16[96,4096]{1,0:T(8,128)(2,1)} custom-call(bf16[384,4096]{1,0:T(8,128)(2,1)} %x_ref.1, f32[1,4096]{1,0:T(1,128)} %bitcast.6, f32[4,128]{1,0:T(4,128)} %constant.2.clone.fixed_ref, f32[1,64]{1,0:T(1,128)} %bitcast.7, f32[1,64]{1,0:T(1,128)} %bitcast.8, f32[1,64]{1,0:T(1,128)} %bitcast.9, f32[1,64]{1,0:T(1,128)} %bitcast.10, ...), custom_call_target="tpu_custom_call" | custom-call | tf_op jit(solution)/shard_map/pallas_call | solution.py:563
  152.8 2.1 %copy.18 = bf16[96,4096]{1,0:T(8,128)(2,1)} copy(bf16[96,4096]{1,0:T(8,128)(2,1)} %shard_map.154) | data formatting | bytes 1572864
where the time goes:
time: 155 us
  Pallas kernels  153 us (99%)
  local copies, waits for them, and re-layouts  2.06 us (1%)
    pallas_call x1, Pallas kernels, local(): pl.pallas_call(functools.partial(layer_kernel, (q_heads, kv_heads, len(we...  153 us

commit v1 on v0

--- a/solution.py
+++ b/solution.py
@@ -516,7 +516,7 @@
     keys.finish()
 
 
-def local(
+def local_ring(
     tokens_in,
     norm_gain,
     window_query,
@@ -597,6 +597,695 @@
     )(tokens_in, norm_gain[None, :], fixed, *gains, sink_logit[None, :], *weights, window_out, dense_out)
 
 
+KINDS = 4
+SHARED = (True, True, False, False)
+ROWS = 128
+
+
+def pair_kernel(sizes, *refs):
+    gain_ref, fixed_ref, g0, g1, g2, g3, sink_ref, x_hbm = refs[:8]
+    weights, outs, out_hbm = refs[8:14], refs[14:16], refs[16]
+    run_pairs(sizes, gain_ref, fixed_ref, (g0, g1, g2, g3), sink_ref, x_hbm, weights, outs, out_hbm, *refs[17:])
+
+
+def run_pairs(
+    sizes, gain_ref, fixed_ref, head_gains, sink_ref, x_hbm, weights, outs, out_hbm,
+    small_ref, tables_ref, xv, xn, wbuf, wo, proj, kvd, ext, extm, qc, qm, qs, att, part, dbuf, xsend, xrecv, ostage,
+    load_sem, store_sem, zs, zr, ys, yr, wis, wzr, wos, wys, wyr,
+    xzs, xzr, xxs, xxr, xds, xdr, xes, xer, kis, kos, kr, es, er, qsn, qr, ds, dr, rxs, rxr,
+):
+    q_heads, kv_heads = sizes
+    n, s = lax.axis_size("sp"), lax.axis_index("sp")
+    n_tp, t = lax.axis_size("tp"), lax.axis_index("tp")
+    g = lax.axis_index("grp")
+    length, width = xv.shape
+    depth, cols = wbuf.shape[2], wbuf.shape[3]
+    out_rows, out_cols = wo.shape[1], wo.shape[2]
+    share = length // n_tp
+    chunks, out_chunks = zs.shape[3], wis.shape[2]
+    low = 2 * s < n
+    high = jnp.logical_not(low)
+    inner = (s > 0) & (s < n - 1)
+    outer = jnp.logical_not(inner)
+    step = jnp.where(low, 1, -1)
+    inward = s + step
+    outward = lax.rem(s - step + n, n)
+    core, chip = lax.rem(t, 2), t // 2
+    twin = t + 1 - 2 * core
+    across = lax.rem(t + 2, n_tp)
+    diagonal = lax.rem(twin + 2, n_tp)
+
+    def place_of(j):
+        if j == 0:
+            return s
+        return jnp.where(inner, (s - step, s - step, s + step, s + 2 * step)[j], s + j * step)
+
+    sent = []
+
+    def remote(when, ends):
+        def build():
+            src, dst, send, recv, peer = ends()
+            return pltpu.make_async_remote_copy(
+                src_ref=src, dst_ref=dst, send_sem=send, recv_sem=recv, device_id=peer, device_id_type=MESH
+            )
+
+        sent.append((when, build))
+        build().start()
+
+    def landed(ref, sem, peer):
+        pltpu.make_async_remote_copy(
+            src_ref=ref, dst_ref=ref, send_sem=sem, recv_sem=sem, device_id=peer, device_id_type=MESH
+        ).wait_recv()
+
+    z_in, z_out, y_peer = {"sp": inward}, {"sp": outward}, {"grp": 1 - g}
+
+    half = depth // HALVES
+    size = half // chunks
+
+    def w_at(k, slot, rel, c):
+        h = g if rel == 0 else 1 - g
+        return wbuf.at[k, slot, pl.ds(pl.multiple_of(h * half + c * size, size), size)]
+
+    def w_inward(role, k, slot, rel, c):
+        to = 1 if role == "outer" else slot + 2
+        remote(role, lambda: (
+            w_at(k, slot, rel, c), w_at(k, to, rel, c), zs.at[k, slot, rel, c], zr.at[k, to, rel, c], z_in
+        ))
+
+    def w_landed(k, slot, rel, c):
+        landed(w_at(k, slot, rel, c), zr.at[k, slot, rel, c], z_out if slot == 1 else z_in)
+
+    def w_twin(k, slot, c):
+        remote("inner", lambda: (
+            w_at(k, slot, 0, c), w_at(k, slot, 0, c), ys.at[k, slot, c], yr.at[k, slot, c], y_peer
+        ))
+
+    def w_twin_landed(k, slot, c):
+        landed(w_at(k, slot, 1, c), yr.at[k, slot, c], y_peer)
+
+    out_half = out_cols // HALVES
+    out_size = out_half // out_chunks
+
+    def o_at(slot, rel, c):
+        h = g if rel == 0 else 1 - g
+        return wo.at[slot, :, pl.ds(pl.multiple_of(h * out_half + c * out_size, out_size), out_size)]
+
+    def o_inward(role, slot, rel, c):
+        to = 1 if role == "outer" else slot + 2
+        remote(role, lambda: (
+            o_at(slot, rel, c), o_at(to, rel, c), wis.at[slot, rel, c], wzr.at[to, rel, c], z_in
+        ))
+
+    def o_outward(slot, c):
+        to = 1 if slot == 0 else slot
+        remote("inner", lambda: (
+            o_at(slot, 0, c), o_at(to, 0, c), wos.at[slot, c], wzr.at[to, 0, c], z_out
+        ))
+
+    def o_landed(slot, rel, c, peer):
+        landed(o_at(slot, rel, c), wzr.at[slot, rel, c], peer)
+
+    def o_twin(role, slot, c):
+        remote(role, lambda: (o_at(slot, 0, c), o_at(slot, 0, c), wys.at[slot, c], wyr.at[slot, c], y_peer))
+
+    def o_twin_landed(slot, c):
+        landed(o_at(slot, 1, c), wyr.at[slot, c], y_peer)
+
+    def x_rows(quarter):
+        return pl.ds(pl.multiple_of(length + quarter * share, share), share)
+
+    def x_cols(p):
+        return pl.ds(p * depth, depth)
+
+    def x_relay(p):
+        def piece():
+            return xn.at[x_rows(t), x_cols(p)]
+
+        landed(piece(), xzr.at[p], z_out)
+        remote("inner", lambda: (piece(), piece(), xxs.at[p], xxr.at[p], {"tp": across}))
+        remote("inner", lambda: (piece(), piece(), xds.at[p], xdr.at[p], {"tp": twin}))
+
+    def x_pass(p):
+        def piece():
+            return xn.at[x_rows(across), x_cols(p)]
+
+        landed(piece(), xxr.at[p], {"tp": across})
+        remote("inner", lambda: (piece(), piece(), xes.at[p], xer.at[p], {"tp": twin}))
+
+    def x_all(p):
+        landed(xn.at[x_rows(twin), x_cols(p)], xdr.at[p], {"tp": twin})
+        landed(xn.at[x_rows(diagonal), x_cols(p)], xer.at[p], {"tp": twin})
+
+    kv_cols = cols // 2
+    loads = []
+
+    def load(src, dst):
+        copy = pltpu.make_async_copy(src, dst, load_sem.at[len(loads)])
+        loads.append(copy)
+        copy.start()
+
+    wq, dq, dk, dv, wk, wv = weights
+    load(dk, wbuf.at[0, 0, :, 0:kv_cols])
+    load(dv, wbuf.at[0, 0, :, kv_cols:cols])
+    load(x_hbm, xv)
+    load(dq, wbuf.at[1, 0])
+    load(wk, wbuf.at[2, 0, :, 0:kv_cols])
+    load(wv, wbuf.at[2, 0, :, kv_cols:cols])
+    load(wq, wbuf.at[3, 0])
+    rows_of = outs[0].shape[0]
+    load(outs[0], wo.at[0, 0:rows_of])
+    load(outs[1], wo.at[0, rows_of:out_rows])
+    greet()
+
+    all_chunks, all_out = range(chunks), range(out_chunks)
+    loads[0].wait()
+    loads[1].wait()
+
+    for role, test in (("inner", inner), ("outer", outer)):
+
+        @pl.when(test)
+        def _():
+            for c in all_chunks:
+                w_inward(role, 0, 0, 0, c)
+
+    for k, ref in enumerate(head_gains):
+        small_ref[k : k + 1, :] = jnp.concatenate([ref[...], ref[...]], axis=1)
+    small_ref[4:8, :] = fixed_ref[...]
+    loads[2].wait()
+
+    def normalize(first, count):
+        stripe = 16
+
+        @pl.loop(0, count // stripe)
+        def _(i):
+            at = pl.multiple_of(i * stripe, stripe)
+            values = xv[pl.ds(first + at, stripe), :].astype(jnp.float32)
+            mean = jnp.mean(values * values, axis=-1, keepdims=True)
+            xn[pl.ds(at, stripe), :] = (values * lax.rsqrt(mean + EPS) * gain_ref[...]).astype(jnp.bfloat16)
+
+    band = 64
+
+    def tables(first, count):
+        @pl.loop(0, count // band)
+        def _(i):
+            at = pl.multiple_of(i * band, band) + first
+            rows = pl.ds(at, band)
+            shape = (band, LANES)
+            base = jnp.where(at < length, s * length + at, (s - step) * length + at - length)
+            place = lax.broadcasted_iota(jnp.int32, shape, 0) + base
+            lane = lax.broadcasted_iota(jnp.int32, shape, 1)
+            spot = jnp.where(lax.rem(lane, HD) < HD // 2, place // GRID_W, lax.rem(place, GRID_W))
+            for k, where in enumerate((place, spot)):
+                angles = where.astype(jnp.float32) * small_ref[4 + k : 5 + k, :]
+                tables_ref[2 * k, rows, :] = jnp.cos(angles)
+                tables_ref[2 * k + 1, rows, :] = jnp.sin(angles) * small_ref[6 + k : 7 + k, :]
+
+    def project(k, j):
+        at = pl.multiple_of(place_of(j) * depth, depth)
+
+        @pl.loop(0, 2)
+        def _(i):
+            rows = pl.ds(pl.multiple_of(i * length, length), length)
+            found = jnp.dot(xn[rows, pl.ds(at, depth)], wbuf[k, j], preferred_element_type=jnp.float32)
+            proj[rows, :] = found if j == 0 else proj[rows, :] + found
+
+    den_q, den_k, win_q, win_k = (2, 1, 16), (3, 1, 16), (0, 0, 32), (1, 0, 32)
+    plans = ((den_k, None), (den_q, den_q), (win_k, None), (win_q, win_q))
+    targets = ((kvd.at[0], kvd.at[1]), (qc.at[0], qm.at[0]), (ext.at[pl.ds(WINDOW, length)], extm), (qc.at[1], qm.at[1]))
+
+    def finished(k):
+        for side, target in enumerate(targets[k]):
+
+            @pl.loop(0, length // ROWS)
+            def _(i):
+                at = pl.multiple_of(i * ROWS, ROWS)
+                rows = pl.ds(side * length + at, ROWS)
+                for tile in range(cols // LANES):
+                    lanes = pl.ds(tile * LANES, LANES)
+                    kind = plans[k][tile * 2 * LANES // cols]
+                    value = proj[rows, lanes]
+                    if kind is not None:
+                        value = head_tile(
+                            value, (kind, kind), small_ref,
+                            [tables_ref.at[m][rows, :] for m in range(4)],
+                        )
+                        if k % 2:
+                            value = value * HD ** (-0.5)
+                    target[pl.ds(at, ROWS), lanes] = value.astype(jnp.bfloat16)
+
+    def mates(k, c):
+        w_landed(k, 1, 0, c)
+        w_inward("inner", k, 1, 0, c)
+        if SHARED[k]:
+            w_twin(k, 1, c)
+
+    def crossing(k, slot, c):
+        w_landed(k, slot, 0, c)
+        w_twin(k, slot, c)
+
+    def mate_ready(k):
+        for c in all_chunks:
+            if SHARED[k]:
+                w_twin_landed(k, 1, c)
+            else:
+                w_landed(k, 1, 1, c)
+
+    def twin_ready(k, slot):
+        for c in all_chunks:
+            w_twin_landed(k, slot, c)
+
+    def o_mates(c):
+        o_landed(1, 0, c, z_out)
+        o_inward("inner", 1, 0, c)
+
+    def o_crossing(slot, c):
+        o_landed(slot, 0, c, z_in)
+        o_outward(slot, c)
+        o_twin("inner", slot, c)
+
+    def o_outer(slot, c):
+        o_landed(slot, 0, c, z_in)
+        o_twin("outer", slot, c)
+
+    def edge(first):
+        return pl.ds(jnp.where(first, WINDOW, length), WINDOW)
+
+    def halo_at(leading):
+        return pl.ds(jnp.where(leading, 0, WINDOW + length), WINDOW)
+
+    def kv_landed(j, peer):
+        landed(kvd.at[j], kr.at[j], peer)
+
+    def kv_outward(j):
+        remote("inner", lambda: (kvd.at[j], kvd.at[j], kos.at[j], kr.at[j], z_out))
+
+    def kv_inward(j):
+        remote("inner", lambda: (kvd.at[j], kvd.at[j + 2], kis.at[j], kr.at[j + 2], z_in))
+
+    def x_inward(p):
+        remote("outer", lambda: (
+            xn.at[0:share, x_cols(p)], xn.at[x_rows(t), x_cols(p)], xzs.at[p], xzr.at[p], z_in
+        ))
+
+    def q_outward(a):
+        remote("inner", lambda: (qm.at[a], qc.at[a], qsn.at[a], qr.at[a], z_out))
+
+    @pl.when(outer)
+    def _():
+        normalize(t * share, share)
+        for p in range(width // depth):
+            x_inward(p)
+        for one in loads[3:]:
+            one.wait()
+        for k in range(1, KINDS):
+            for rel in range(1 if SHARED[k] else 2):
+                for c in all_chunks:
+                    w_inward("outer", k, 0, rel, c)
+        for rel in range(2):
+            for c in all_out:
+                o_inward("outer", 0, rel, c)
+        for c in all_out:
+            o_outer(1, c)
+        none = jnp.zeros((WINDOW, cols), jnp.bfloat16)
+        ext[halo_at(low), :] = none
+        for j in range(2):
+            kv_landed(j, z_in)
+        landed(qc.at[0], qr.at[0], z_in)
+        for j in range(2, 4):
+            kv_landed(j, z_in)
+
+    @pl.when(inner)
+    def _():
+        for one in loads[3:]:
+            one.wait()
+        for c in all_out:
+            o_outward(0, c)
+        normalize(0, length)
+        for c in all_chunks:
+            mates(0, c)
+            crossing(0, 2, c)
+        for k in range(1, KINDS):
+            for c in all_chunks:
+                w_inward("inner", k, 0, 0, c)
+        tables(0, length)
+        for c in all_chunks:
+            crossing(0, 3, c)
+        x_relay(0)
+        tables(length, length)
+        crossing(1, 2, 0)
+        x_relay(1)
+        crossing(1, 2, 1)
+        x_pass(0)
+        x_relay(2)
+        crossing(2, 2, 0)
+        x_pass(1)
+        x_relay(3)
+        crossing(2, 2, 1)
+        x_pass(2)
+        crossing(3, 2, 0)
+        mates(1, 0)
+        x_pass(3)
+        crossing(3, 2, 1)
+        mates(1, 1)
+        for p in range(width // depth):
+            x_all(p)
+        project(0, 0)
+        mate_ready(0)
+        project(0, 1)
+        twin_ready(0, 2)
+        project(0, 2)
+        twin_ready(0, 3)
+        project(0, 3)
+        finished(0)
+        for j in range(2):
+            kv_inward(j)
+            kv_outward(j)
+        for c in all_chunks:
+            mates(2, c)
+            crossing(1, 3, c)
+        project(1, 0)
+        mate_ready(1)
+        project(1, 1)
+        twin_ready(1, 2)
+        project(1, 2)
+        twin_ready(1, 3)
+        project(1, 3)
+        finished(1)
+        q_outward(0)
+        for j in range(2, 4):
+            kv_landed(j, z_in)
+            kv_outward(j)
+        for c in all_chunks:
+            mates(3, c)
+        for c in all_out:
+            o_inward("inner", 0, 0, c)
+        project(2, 0)
+        for c in all_chunks:
+            crossing(2, 3, c)
+
+    group = q_heads // kv_heads
+
+    def spot_of(head):
+        return head // 2, head % 2
+
+    q_tiles = q_heads * HD // LANES
+
+    def expand(a):
+        for i in range(q_tiles):
+            tile = qc[a, :, i * LANES : (i + 1) * LANES].astype(jnp.float32)
+            for b in range(2):
+                head = 2 * i + b
+                side = spot_of(head // group)[1]
+                moved = tile if side == b else pltpu.roll(tile, HD, 1)
+                zero = jnp.zeros_like(moved)
+                kept = by_half(moved, zero) if side == 0 else by_half(zero, moved)
+                qs[head] = kept.astype(jnp.bfloat16)
+
+    total_len = length * n
+
+    def joined(results, heads):
+        placed = []
+        for b in range(2):
+            side = spot_of(kv_heads + heads[b] // group)[1]
+            placed.append(results[b] if side == b else pltpu.roll(results[b], HD, 1))
+        return by_half(placed[0], placed[1]).astype(jnp.bfloat16)
+
+    def tile_of(head):
+        return pl.ds(spot_of(head)[0] * LANES, LANES)
+
+    nt = (((1,), (1,)), ((), ()))
+    pairs = q_heads // 2
+
+    def windowed(pair):
+        @pl.loop(0, length // WINDOW)
+        def _(b):
+            base = pl.multiple_of(b * WINDOW, WINDOW)
+            rows = pl.ds(base, WINDOW)
+            near = pl.ds(base, 3 * WINDOW)
+            shape = (WINDOW, 3 * WINDOW)
+            at = lax.broadcasted_iota(jnp.int32, shape, 1) - WINDOW
+            away = at - lax.broadcasted_iota(jnp.int32, shape, 0)
+            pos = at + (s * length + base)
+            valid = (away <= WINDOW) & (away >= -WINDOW) & (pos >= 0) & (pos < total_len)
+            results = []
+            for head in (2 * pair, 2 * pair + 1):
+                key = ext[near, tile_of(head // group)]
+                value = ext[near, tile_of(kv_heads + head // group)]
+                scores = lax.dot_general(qs[head, rows, :], key, nt, preferred_element_type=jnp.float32)
+                scores = jnp.where(valid, scores, -jnp.inf)
+                floor = sink_ref[0, head]
+                top = jnp.maximum(jnp.max(scores, axis=-1, keepdims=True), floor)
+                expon = jnp.exp(scores - top)
+                total = jnp.sum(expon, axis=-1, keepdims=True) + jnp.exp(floor - top)
+                weight = (expon / total).astype(jnp.bfloat16)
+                results.append(jnp.dot(weight, value, preferred_element_type=jnp.float32))
+            att[rows, pair * LANES : (pair + 1) * LANES] = joined(results, (2 * pair, 2 * pair + 1))
+
+    def dense(pair):
+        @pl.loop(0, length // LANES)
+        def _(b):
+            rows = pl.ds(pl.multiple_of(b * LANES, LANES), LANES)
+            results = []
+            for head in (2 * pair, 2 * pair + 1):
+                key = kvd[:, :, tile_of(head // group)].reshape(total_len, LANES)
+                value = kvd[:, :, tile_of(kv_heads + head // group)].reshape(total_len, LANES)
+                scores = lax.dot_general(qs[head, rows, :], key, nt, preferred_element_type=jnp.float32)
+                top = jnp.max(scores, axis=-1, keepdims=True)
+                expon = jnp.exp(scores - top)
+                total = jnp.sum(expon, axis=-1, keepdims=True)
+                summed = jnp.dot(expon.astype(jnp.bfloat16), value, preferred_element_type=jnp.float32)
+                results.append(summed / total)
+            at = (pairs + pair) * LANES
+            att[rows, at : at + LANES] = joined(results, (2 * pair, 2 * pair + 1))
+
+    expand(0)
+    dense(0)
+
+    @pl.when(inner)
+    def _():
+        mate_ready(2)
+        project(2, 1)
+        twin_ready(2, 2)
+        project(2, 2)
+        twin_ready(2, 3)
+        project(2, 3)
+        finished(2)
+        ext[halo_at(low), :] = extm[pl.ds(jnp.where(low, length - WINDOW, 0), WINDOW), :]
+        remote("inner", lambda: (ext.at[edge(high)], ext.at[halo_at(low)], es.at[2], er.at[2], z_in))
+        remote("inner", lambda: (extm, ext.at[pl.ds(WINDOW, length)], es.at[0], er.at[0], z_out))
+        remote("inner", lambda: (ext.at[edge(low)], ext.at[halo_at(high)], es.at[1], er.at[1], z_out))
+        for c in all_out:
+            o_mates(c)
+        for c in all_chunks:
+            crossing(3, 3, c)
+        project(3, 0)
+        mate_ready(3)
+        project(3, 1)
+        twin_ready(3, 2)
+        project(3, 2)
+
+    dense(1)
+
+    @pl.when(outer)
+    def _():
+        landed(ext.at[pl.ds(WINDOW, length)], er.at[0], z_in)
+        landed(ext.at[halo_at(high)], er.at[1], z_in)
+        for c in all_out:
+            o_outer(2, c)
+        landed(qc.at[1], qr.at[1], z_in)
+
+    @pl.when(inner)
+    def _():
+        for c in all_out:
+            o_crossing(2, c)
+        twin_ready(3, 3)
+        project(3, 3)
+        finished(3)
+        q_outward(1)
+        landed(ext.at[halo_at(high)], er.at[2], z_in)
+
+    expand(1)
+    for pair in range(pairs):
+        windowed(pair)
+
+    def span(rel):
+        h = g if rel == 0 else 1 - g
+        return pl.ds(pl.multiple_of(h * out_half, out_half), out_half)
+
+    def part_rows(dest):
+        return pl.ds(pl.multiple_of(dest * share, share), share)
+
+    def emit(j, rel):
+        part[j, :, span(rel)] = jnp.dot(
+            att[...], wo[j, :, span(rel)], preferred_element_type=jnp.float32
+        ).astype(jnp.bfloat16)
+        for i in range(2):
+            exchange(j, rel, i)
+
+    def exchange(j, rel, i):
+        remote("both", lambda: (
+            part.at[j, part_rows(2 * i + 1 - core), span(rel)], dbuf.at[j, i, :, span(rel)],
+            ds.at[j, rel, i], dr.at[j, rel, i], {"tp": twin},
+        ))
+
+    def combine(j, rel):
+        for i in range(2):
+            landed(dbuf.at[j, i, :, span(rel)], dr.at[j, rel, i], {"tp": twin})
+        other = 1 - chip
+        both = (
+            part[j, part_rows(2 * other + core), span(rel)].astype(jnp.float32)
+            + dbuf[j, other, :, span(rel)].astype(jnp.float32)
+        )
+        xsend[j, :, span(rel)] = both.astype(jnp.bfloat16)
+        remote("both", lambda: (
+            xsend.at[j, :, span(rel)], xrecv.at[j, :, span(rel)], rxs.at[j, rel], rxr.at[j, rel], {"tp": across}
+        ))
+
+    def store(j, rel):
+        h = g if rel == 0 else 1 - g
+        at = pl.ds(pl.multiple_of(place_of(j) * out_cols + h * out_half, out_half), out_half)
+        return pltpu.make_async_copy(ostage.at[j, :, span(rel)], out_hbm.at[:, at], store_sem.at[j, rel])
+
+    def settle(j, rel):
+        landed(xrecv.at[j, :, span(rel)], rxr.at[j, rel], {"tp": across})
+        total = (
+            part[j, part_rows(t), span(rel)].astype(jnp.float32)
+            + dbuf[j, chip, :, span(rel)].astype(jnp.float32)
+            + xrecv[j, :, span(rel)].astype(jnp.float32)
+        )
+        ostage[j, :, span(rel)] = total.astype(jnp.bfloat16)
+        store(j, rel).start()
+
+    def arrive(j, rel):
+        if (j, rel) == (1, 1):
+
+            @pl.when(inner)
+            def _():
+                for c in all_out:
+                    o_landed(1, 1, c, z_out)
+
+            @pl.when(outer)
+            def _():
+                for c in all_out:
+                    o_twin_landed(1, c)
+
+        elif rel == 1 and j > 1:
+            for c in all_out:
+                o_twin_landed(j, c)
+        elif (j, rel) == (3, 0):
+
+            @pl.when(inner)
+            def _():
+                for c in all_out:
+                    o_crossing(3, c)
+
+            @pl.when(outer)
+            def _():
+                for c in all_out:
+                    o_outer(3, c)
+
+    order = ((0, 0), (0, 1), (1, 0), (2, 0), (2, 1), (3, 0), (1, 1), (3, 1))
+    for i, piece in enumerate(order):
+        arrive(*piece)
+        emit(*piece)
+        if i >= 1:
+            combine(*order[i - 1])
+        if i >= 2:
+            settle(*order[i - 2])
+    combine(*order[-1])
+    settle(*order[-2])
+    settle(*order[-1])
+
+    for role, test in (("inner", inner), ("outer", outer)):
+
+        @pl.when(test)
+        def _():
+            for when, build in sent:
+                if when == role:
+                    build().wait_send()
+
+    for when, build in sent:
+        if when == "both":
+            build().wait_send()
+    for piece in order:
+        store(*piece).wait()
+
+
+def local(*args):
+    tokens_in, norm_gain, wq, wk, wv, wq_gain, wk_gain, sink, dq, dk, dv, dq_gain, dk_gain, w_out, d_out = args
+    length, width = tokens_in.shape
+    n, n_tp = lax.axis_size("sp"), lax.axis_size("tp")
+    depth, cols = wq.shape
+    paired = (
+        n == 4 and n_tp == 4 and wk.shape[1] == LANES and cols == 2 * LANES and depth * n == width
+        and length % (n_tp * 32) == 0 and length % WINDOW == 0
+    )
+    if not paired:
+        return local_ring(*args)
+    q_heads, kv_heads = cols // HD, wk.shape[1] // HD
+    out_rows, out_cols = w_out.shape[0] + d_out.shape[0], w_out.shape[1]
+    share = length // n_tp
+    lane = np.arange(LANES)
+    fixed = np.stack(
+        [THETA ** (-2.0 * (lane % (wide // 2)) / wide) for wide in (HD, HD // 2)]
+        + [np.where(lane % wide < wide // 2, -1.0, 1.0) for wide in (HD, HD // 2)]
+    ).astype(np.float32)
+    gains = [gain[None, :] for gain in (wq_gain, wk_gain, dq_gain, dk_gain)]
+    chunks, out_chunks, pieces = 2, 4, width // depth
+    vmem = pl.BlockSpec(memory_space=pltpu.VMEM)
+    bf16 = jnp.bfloat16
+
+    def sem(*shape):
+        return pltpu.SemaphoreType.DMA(shape)
+
+    return pl.pallas_call(
+        functools.partial(pair_kernel, (q_heads, kv_heads)),
+        out_shape=jax.ShapeDtypeStruct((share, width), bf16),
+        in_specs=[vmem] * 6
+        + [pl.BlockSpec(memory_space=pltpu.SMEM)]
+        + [pl.BlockSpec(memory_space=pl.ANY)] * 9,
+        out_specs=pl.BlockSpec(memory_space=pl.ANY),
+        scratch_shapes=[
+            pltpu.VMEM((8, LANES), jnp.float32),
+            pltpu.VMEM((4, 2 * length, LANES), jnp.float32),
+            pltpu.VMEM((length, width), bf16),
+            pltpu.VMEM((2 * length, width), bf16),
+            pltpu.VMEM((KINDS, n, depth, cols), bf16),
+            pltpu.VMEM((n, out_rows, out_cols), bf16),
+            pltpu.VMEM((2 * length, cols), jnp.float32),
+            pltpu.VMEM((n, length, cols), bf16),
+            pltpu.VMEM((length + 2 * WINDOW, cols), bf16),
+            pltpu.VMEM((length, cols), bf16),
+            pltpu.VMEM((2, length, cols), bf16),
+            pltpu.VMEM((2, length, cols), bf16),
+            pltpu.VMEM((q_heads, length, LANES), bf16),
+            pltpu.VMEM((length, out_rows), bf16),
+            pltpu.VMEM((n, length, out_cols), bf16),
+            pltpu.VMEM((n, 2, share, out_cols), bf16),
+            pltpu.VMEM((n, share, out_cols), bf16),
+            pltpu.VMEM((n, share, out_cols), bf16),
+            pltpu.VMEM((n, share, out_cols), bf16),
+            sem(9),
+            sem(n, HALVES),
+            sem(KINDS, 2, HALVES, chunks),
+            sem(KINDS, n, HALVES, chunks),
+            sem(KINDS, n, chunks),
+            sem(KINDS, n, chunks),
+            sem(2, HALVES, out_chunks),
+            sem(n, HALVES, out_chunks),
+            sem(n, out_chunks),
+            sem(n, out_chunks),
+            sem(n, out_chunks),
+        ]
+        + [sem(pieces)] * 8
+        + [sem(2), sem(n), sem(n), sem(3), sem(3), sem(2), sem(2)]
+        + [sem(n, HALVES, 2), sem(n, HALVES, 2), sem(n, HALVES), sem(n, HALVES)],
+        compiler_params=pltpu.CompilerParams(
+            collective_id=0, has_side_effects=True, vmem_limit_bytes=62 * 1024 * 1024
+        ),
+    )(norm_gain[None, :], fixed, *gains, sink[None, :], tokens_in, wq, dq, dk, dv, wk, wv, w_out, d_out)
+
+
 def solution(mesh):
     return jax.shard_map(
         local,

time: 155 us -> 135 us (0.87)
  Pallas kernels: 153 us -> 133 us
    pallas_call x1, Pallas kernels: 153 us -> 133 us  [local(): pl.pallas_call(functools.partial(pair_kernel, (q_heads, kv_heads)), out_s...]
where the time goes in v1:
time: 135 us
  Pallas kernels  133 us (99%)
  local copies, waits for them, and re-layouts  2.06 us (2%)
    pallas_call x1, Pallas kernels, local(): pl.pallas_call(functools.partial(pair_kernel, (q_heads, kv_heads)), out_s...  133 us

profile of v1, /device:TPU:0, one launch (start us, length us, event | category | flops | bytes accessed | tf_op | source)
XLA Modules:
  0.0 134.9 jit_solution(12995441299029112714)
XLA Ops:
  0.0 132.8 %shard_map.154 = bf16[96,4096]{1,0:T(8,128)(2,1)} custom-call(f32[1,4096]{1,0:T(1,128)} %bitcast.6, f32[4,128]{1,0:T(4,128)} %constant.2.clone.refs_1_, f32[1,64]{1,0:T(1,128)} %bitcast.7, f32[1,64]{1,0:T(1,128)} %bitcast.8, f32[1,64]{1,0:T(1,128)} %bitcast.9, f32[1,64]{1,0:T(1,128)} %bitcast.10, f32[1,4]{1,0:T(1,128)} %bitcast.11, ...), custom_call_target="tpu_custom_call" | custom-call | tf_op jit(solution)/shard_map/pallas_call | solution.py:1241
  132.8 2.1 %copy.18 = bf16[96,4096]{1,0:T(8,128)(2,1)} copy(bf16[96,4096]{1,0:T(8,128)(2,1)} %shard_map.154) | data formatting | bytes 1572864

commit v2 on v1

--- a/solution.py
+++ b/solution.py
@@ -598,9 +598,7 @@
 
 
 KINDS = 4
-SHARED = (True, True, False, False)
-ROWS = 128
-
+SHARED = (True, False, False, False)
 
 def pair_kernel(sizes, *refs):
     gain_ref, fixed_ref, g0, g1, g2, g3, sink_ref, x_hbm = refs[:8]
@@ -610,9 +608,9 @@
 
 def run_pairs(
     sizes, gain_ref, fixed_ref, head_gains, sink_ref, x_hbm, weights, outs, out_hbm,
-    small_ref, tables_ref, xv, xn, wbuf, wo, proj, kvd, ext, extm, qc, qm, qs, att, part, dbuf, xsend, xrecv, ostage,
+    small_ref, tables_ref, xv, xn, wbuf, wo, proj, kvd, ext, qs, att, part, dbuf, xsend, xrecv, ostage,
     load_sem, store_sem, zs, zr, ys, yr, wis, wzr, wos, wys, wyr,
-    xzs, xzr, xxs, xxr, xds, xdr, xes, xer, kis, kos, kr, es, er, qsn, qr, ds, dr, rxs, rxr,
+    xzs, xzr, xxs, xxr, xds, xdr, xes, xer, kis, kr, hs, hr, ats, atr, ds, dr, rxs, rxr,
 ):
     q_heads, kv_heads = sizes
     n, s = lax.axis_size("sp"), lax.axis_index("sp")
@@ -800,38 +798,43 @@
                 tables_ref[2 * k, rows, :] = jnp.cos(angles)
                 tables_ref[2 * k + 1, rows, :] = jnp.sin(angles) * small_ref[6 + k : 7 + k, :]
 
-    def project(k, j):
+    def project(k, j, sides=(0, 1)):
         at = pl.multiple_of(place_of(j) * depth, depth)
 
-        @pl.loop(0, 2)
+        @pl.loop(sides[0], sides[-1] + 1)
         def _(i):
             rows = pl.ds(pl.multiple_of(i * length, length), length)
             found = jnp.dot(xn[rows, pl.ds(at, depth)], wbuf[k, j], preferred_element_type=jnp.float32)
-            proj[rows, :] = found if j == 0 else proj[rows, :] + found
+            proj[k % 2, rows, :] = found if j == 0 else proj[k % 2, rows, :] + found
 
     den_q, den_k, win_q, win_k = (2, 1, 16), (3, 1, 16), (0, 0, 32), (1, 0, 32)
     plans = ((den_k, None), (den_q, den_q), (win_k, None), (win_q, win_q))
-    targets = ((kvd.at[0], kvd.at[1]), (qc.at[0], qm.at[0]), (ext.at[pl.ds(WINDOW, length)], extm), (qc.at[1], qm.at[1]))
-
-    def finished(k):
-        for side, target in enumerate(targets[k]):
-
-            @pl.loop(0, length // ROWS)
-            def _(i):
-                at = pl.multiple_of(i * ROWS, ROWS)
-                rows = pl.ds(side * length + at, ROWS)
-                for tile in range(cols // LANES):
-                    lanes = pl.ds(tile * LANES, LANES)
-                    kind = plans[k][tile * 2 * LANES // cols]
-                    value = proj[rows, lanes]
-                    if kind is not None:
-                        value = head_tile(
-                            value, (kind, kind), small_ref,
-                            [tables_ref.at[m][rows, :] for m in range(4)],
-                        )
-                        if k % 2:
-                            value = value * HD ** (-0.5)
-                    target[pl.ds(at, ROWS), lanes] = value.astype(jnp.bfloat16)
+    group = q_heads // kv_heads
+    pairs = q_heads // 2
+
+    def finished(k, side):
+        rows = pl.ds(side * length, length)
+        for tile in range(cols // LANES):
+            lanes = pl.ds(tile * LANES, LANES)
+            kind = plans[k][tile * 2 * LANES // cols]
+            value = proj[k % 2, rows, lanes]
+            if kind is not None:
+                value = head_tile(
+                    value, (kind, kind), small_ref, [tables_ref.at[m][rows, :] for m in range(4)]
+                )
+            if k % 2:
+                value = value * HD ** (-0.5)
+                zero = jnp.zeros_like(value)
+                for b in range(2):
+                    head = 2 * tile + b
+                    half_of = head // group % 2
+                    moved = value if half_of == b else pltpu.roll(value, HD, 1)
+                    kept = by_half(moved, zero) if half_of == 0 else by_half(zero, moved)
+                    qs[k // 2, side, head] = kept.astype(jnp.bfloat16)
+            elif k == 0:
+                kvd[side, :, lanes] = value.astype(jnp.bfloat16)
+            else:
+                ext[side, pl.ds(WINDOW, length), lanes] = value.astype(jnp.bfloat16)
 
     def mates(k, c):
         w_landed(k, 1, 0, c)
@@ -873,11 +876,19 @@
     def halo_at(leading):
         return pl.ds(jnp.where(leading, 0, WINDOW + length), WINDOW)
 
-    def kv_landed(j, peer):
-        landed(kvd.at[j], kr.at[j], peer)
-
-    def kv_outward(j):
-        remote("inner", lambda: (kvd.at[j], kvd.at[j], kos.at[j], kr.at[j], z_out))
+    def halo_inward():
+        remote("inner", lambda: (ext.at[0, edge(high)], ext.at[0, halo_at(low)], hs.at[0], hr.at[0], z_in))
+
+    def halo_landed():
+        landed(ext.at[0, halo_at(high)], hr.at[0], z_in)
+
+    def halo_local():
+        ext[0, halo_at(low), :] = ext[1, edge(high), :]
+        ext[1, halo_at(high), :] = ext[0, edge(low), :]
+        ext[1, halo_at(low), :] = jnp.zeros((WINDOW, cols), jnp.bfloat16)
+
+    def kv_landed(j):
+        landed(kvd.at[j], kr.at[j], z_in)
 
     def kv_inward(j):
         remote("inner", lambda: (kvd.at[j], kvd.at[j + 2], kis.at[j], kr.at[j + 2], z_in))
@@ -887,8 +898,69 @@
             xn.at[0:share, x_cols(p)], xn.at[x_rows(t), x_cols(p)], xzs.at[p], xzr.at[p], z_in
         ))
 
-    def q_outward(a):
-        remote("inner", lambda: (qm.at[a], qc.at[a], qsn.at[a], qr.at[a], z_out))
+    def att_at(side, i):
+        return att.at[side, :, i * LANES : (i + 1) * LANES]
+
+    def att_outward(i):
+        remote("inner", lambda: (att_at(1, i), att_at(0, i), ats.at[i], atr.at[i], z_out))
+
+    def att_landed(i):
+        landed(att_at(0, i), atr.at[i], z_in)
+
+    def joined(results, pair):
+        side = (kv_heads + pair * 2 // group) % 2
+        placed = [results[b] if side == b else pltpu.roll(results[b], HD, 1) for b in range(2)]
+        return by_half(placed[0], placed[1]).astype(jnp.bfloat16)
+
+    def tile_of(head):
+        return pl.ds(head // 2 * LANES, LANES)
+
+    nt = (((1,), (1,)), ((), ()))
+    total_len = length * n
+
+    def windowed(side, pair):
+        start = (s if side == 0 else s - step) * length
+        shape = (2 * WINDOW, 3 * WINDOW)
+        row = lax.rem(lax.broadcasted_iota(jnp.int32, shape, 0), WINDOW)
+        at = lax.broadcasted_iota(jnp.int32, shape, 1) - WINDOW
+        near_by = (at - row <= WINDOW) & (at - row >= -WINDOW)
+        first = lax.broadcasted_iota(jnp.int32, (2 * WINDOW, 1), 0) < WINDOW
+        floor = jnp.where(first, sink_ref[0, 2 * pair], sink_ref[0, 2 * pair + 1])
+        blocks = range(length // WINDOW)
+        near = [pl.ds(b * WINDOW, 3 * WINDOW) for b in blocks]
+        rows = [pl.ds(b * WINDOW, WINDOW) for b in blocks]
+        scores, expon, total = [], [], []
+        for b in blocks:
+            key = ext[side, near[b], tile_of(2 * pair // group)]
+            query = qs[1, side, 2 * pair : 2 * pair + 2, rows[b], :].reshape(2 * WINDOW, LANES)
+            pos = at + (start + b * WINDOW)
+            valid = near_by & (pos >= 0) & (pos < total_len)
+            found = lax.dot_general(query, key, nt, preferred_element_type=jnp.float32)
+            scores.append(jnp.where(valid, found, -jnp.inf))
+        tops = [jnp.maximum(jnp.max(score, axis=-1, keepdims=True), floor) for score in scores]
+        for score, top in zip(scores, tops):
+            expon.append(jnp.exp(score - top))
+            total.append(jnp.sum(expon[-1], axis=-1, keepdims=True) + jnp.exp(floor - top))
+        for b in blocks:
+            value = ext[side, near[b], tile_of(kv_heads + 2 * pair // group)]
+            weight = (expon[b] / total[b]).astype(jnp.bfloat16)
+            found = jnp.dot(weight, value, preferred_element_type=jnp.float32)
+            att[side, rows[b], pair * LANES : (pair + 1) * LANES] = joined((found[:WINDOW], found[WINDOW:]), pair)
+
+    def dense(side, pair):
+        @pl.loop(0, length // LANES)
+        def _(b):
+            rows = pl.ds(pl.multiple_of(b * LANES, LANES), LANES)
+            key = kvd[:, :, tile_of(2 * pair // group)].reshape(total_len, LANES)
+            value = kvd[:, :, tile_of(kv_heads + 2 * pair // group)].reshape(total_len, LANES)
+            query = qs[0, side, 2 * pair : 2 * pair + 2, rows, :].reshape(2 * LANES, LANES)
+            scores = lax.dot_general(query, key, nt, preferred_element_type=jnp.float32)
+            top = jnp.max(scores, axis=-1, keepdims=True)
+            expon = jnp.exp(scores - top)
+            total = jnp.sum(expon, axis=-1, keepdims=True)
+            summed = jnp.dot(expon.astype(jnp.bfloat16), value, preferred_element_type=jnp.float32) / total
+            at = (pairs + pair) * LANES
+            att[side, rows, at : at + LANES] = joined((summed[:LANES], summed[LANES:]), pair)
 
     @pl.when(outer)
     def _():
@@ -897,22 +969,16 @@
             x_inward(p)
         for one in loads[3:]:
             one.wait()
-        for k in range(1, KINDS):
-            for rel in range(1 if SHARED[k] else 2):
-                for c in all_chunks:
-                    w_inward("outer", k, 0, rel, c)
+        for k, rel in ((1, 0), (2, 0), (1, 1), (3, 0), (2, 1), (3, 1)):
+            for c in all_chunks:
+                w_inward("outer", k, 0, rel, c)
         for rel in range(2):
             for c in all_out:
                 o_inward("outer", 0, rel, c)
         for c in all_out:
             o_outer(1, c)
-        none = jnp.zeros((WINDOW, cols), jnp.bfloat16)
-        ext[halo_at(low), :] = none
-        for j in range(2):
-            kv_landed(j, z_in)
-        landed(qc.at[0], qr.at[0], z_in)
-        for j in range(2, 4):
-            kv_landed(j, z_in)
+        for i in range(pairs, 2 * pairs):
+            att_landed(i)
 
     @pl.when(inner)
     def _():
@@ -941,6 +1007,13 @@
         x_pass(1)
         x_relay(3)
         crossing(2, 2, 1)
+        mate_ready(0)
+        for j in range(2, 4):
+            twin_ready(0, j)
+        for j in range(4):
+            project(0, j, (0,))
+        finished(0, 0)
+        kv_inward(0)
         x_pass(2)
         crossing(3, 2, 0)
         mates(1, 0)
@@ -949,252 +1022,194 @@
         mates(1, 1)
         for p in range(width // depth):
             x_all(p)
-        project(0, 0)
-        mate_ready(0)
-        project(0, 1)
-        twin_ready(0, 2)
-        project(0, 2)
-        twin_ready(0, 3)
-        project(0, 3)
-        finished(0)
-        for j in range(2):
-            kv_inward(j)
-            kv_outward(j)
-        for c in all_chunks:
-            mates(2, c)
-            crossing(1, 3, c)
+        for j in range(4):
+            project(0, j, (1,))
+        finished(0, 1)
+        kv_inward(1)
         project(1, 0)
+        twin_ready(1, 2)
+        project(1, 2)
+        mates(2, 0)
+        crossing(1, 3, 0)
+        project(2, 0)
+        mates(2, 1)
+        crossing(1, 3, 1)
+        twin_ready(2, 2)
+        project(2, 2)
         mate_ready(1)
         project(1, 1)
-        twin_ready(1, 2)
-        project(1, 2)
         twin_ready(1, 3)
         project(1, 3)
-        finished(1)
-        q_outward(0)
-        for j in range(2, 4):
-            kv_landed(j, z_in)
-            kv_outward(j)
-        for c in all_chunks:
-            mates(3, c)
+        finished(1, 1)
+        finished(1, 0)
+        kv_landed(2)
+        kv_landed(3)
+        crossing(2, 3, 0)
+        mates(3, 0)
+        dense(1, 0)
+        att_outward(pairs)
+        crossing(2, 3, 1)
+        mates(3, 1)
         for c in all_out:
             o_inward("inner", 0, 0, c)
-        project(2, 0)
-        for c in all_chunks:
-            crossing(2, 3, c)
-
-    group = q_heads // kv_heads
-
-    def spot_of(head):
-        return head // 2, head % 2
-
-    q_tiles = q_heads * HD // LANES
-
-    def expand(a):
-        for i in range(q_tiles):
-            tile = qc[a, :, i * LANES : (i + 1) * LANES].astype(jnp.float32)
-            for b in range(2):
-                head = 2 * i + b
-                side = spot_of(head // group)[1]
-                moved = tile if side == b else pltpu.roll(tile, HD, 1)
-                zero = jnp.zeros_like(moved)
-                kept = by_half(moved, zero) if side == 0 else by_half(zero, moved)
-                qs[head] = kept.astype(jnp.bfloat16)
-
-    total_len = length * n
-
-    def joined(results, heads):
-        placed = []
-        for b in range(2):
-            side = spot_of(kv_heads + heads[b] // group)[1]
-            placed.append(results[b] if side == b else pltpu.roll(results[b], HD, 1))
-        return by_half(placed[0], placed[1]).astype(jnp.bfloat16)
-
-    def tile_of(head):
-        return pl.ds(spot_of(head)[0] * LANES, LANES)
-
-    nt = (((1,), (1,)), ((), ()))
-    pairs = q_heads // 2
-
-    def windowed(pair):
-        @pl.loop(0, length // WINDOW)
-        def _(b):
-            base = pl.multiple_of(b * WINDOW, WINDOW)
-            rows = pl.ds(base, WINDOW)
-            near = pl.ds(base, 3 * WINDOW)
-            shape = (WINDOW, 3 * WINDOW)
-            at = lax.broadcasted_iota(jnp.int32, shape, 1) - WINDOW
-            away = at - lax.broadcasted_iota(jnp.int32, shape, 0)
-            pos = at + (s * length + base)
-            valid = (away <= WINDOW) & (away >= -WINDOW) & (pos >= 0) & (pos < total_len)
-            results = []
-            for head in (2 * pair, 2 * pair + 1):
-                key = ext[near, tile_of(head // group)]
-                value = ext[near, tile_of(kv_heads + head // group)]
-                scores = lax.dot_general(qs[head, rows, :], key, nt, preferred_element_type=jnp.float32)
-                scores = jnp.where(valid, scores, -jnp.inf)
-                floor = sink_ref[0, head]
-                top = jnp.maximum(jnp.max(scores, axis=-1, keepdims=True), floor)
-                expon = jnp.exp(scores - top)
-                total = jnp.sum(expon, axis=-1, keepdims=True) + jnp.exp(floor - top)
-                weight = (expon / total).astype(jnp.bfloat16)
-                results.append(jnp.dot(weight, value, preferred_element_type=jnp.float32))
-            att[rows, pair * LANES : (pair + 1) * LANES] = joined(results, (2 * pair, 2 * pair + 1))
-
-    def dense(pair):
-        @pl.loop(0, length // LANES)
-        def _(b):
-            rows = pl.ds(pl.multiple_of(b * LANES, LANES), LANES)
-            results = []
-            for head in (2 * pair, 2 * pair + 1):
-                key = kvd[:, :, tile_of(head // group)].reshape(total_len, LANES)
-                value = kvd[:, :, tile_of(kv_heads + head // group)].reshape(total_len, LANES)
-                scores = lax.dot_general(qs[head, rows, :], key, nt, preferred_element_type=jnp.float32)
-                top = jnp.max(scores, axis=-1, keepdims=True)
-                expon = jnp.exp(scores - top)
-                total = jnp.sum(expon, axis=-1, keepdims=True)
-                summed = jnp.dot(expon.astype(jnp.bfloat16), value, preferred_element_type=jnp.float32)
-                results.append(summed / total)
-            at = (pairs + pair) * LANES
-            att[rows, at : at + LANES] = joined(results, (2 * pair, 2 * pair + 1))
-
-    expand(0)
-    dense(0)
-
-    @pl.when(inner)
-    def _():
+        dense(1, 1)
+        att_outward(pairs + 1)
         mate_ready(2)
+        crossing(3, 3, 0)
         project(2, 1)
-        twin_ready(2, 2)
-        project(2, 2)
         twin_ready(2, 3)
         project(2, 3)
-        finished(2)
-        ext[halo_at(low), :] = extm[pl.ds(jnp.where(low, length - WINDOW, 0), WINDOW), :]
-        remote("inner", lambda: (ext.at[edge(high)], ext.at[halo_at(low)], es.at[2], er.at[2], z_in))
-        remote("inner", lambda: (extm, ext.at[pl.ds(WINDOW, length)], es.at[0], er.at[0], z_out))
-        remote("inner", lambda: (ext.at[edge(low)], ext.at[halo_at(high)], es.at[1], er.at[1], z_out))
-        for c in all_out:
-            o_mates(c)
-        for c in all_chunks:
-            crossing(3, 3, c)
         project(3, 0)
+        crossing(3, 3, 1)
+        finished(2, 1)
+        finished(2, 0)
+        halo_inward()
+        halo_local()
+        twin_ready(3, 2)
+        project(3, 2)
         mate_ready(3)
         project(3, 1)
-        twin_ready(3, 2)
-        project(3, 2)
-
-    dense(1)
+        o_crossing(2, 0)
+        twin_ready(3, 3)
+        project(3, 3, (1,))
+        finished(3, 1)
+        o_mates(0)
+        windowed(1, 0)
+        att_outward(0)
+        windowed(1, 1)
+        att_outward(1)
+        o_crossing(2, 1)
+        o_mates(1)
+        project(3, 3, (0,))
+        finished(3, 0)
+        halo_landed()
+        o_crossing(2, 2)
+        o_mates(2)
+        windowed(0, 0)
+        windowed(0, 1)
+        o_crossing(2, 3)
+        o_mates(3)
+        dense(0, 0)
+        o_crossing(3, 0)
+        dense(0, 1)
+        o_crossing(3, 1)
 
     @pl.when(outer)
     def _():
-        landed(ext.at[pl.ds(WINDOW, length)], er.at[0], z_in)
-        landed(ext.at[halo_at(high)], er.at[1], z_in)
-        for c in all_out:
-            o_outer(2, c)
-        landed(qc.at[1], qr.at[1], z_in)
-
-    @pl.when(inner)
-    def _():
-        for c in all_out:
-            o_crossing(2, c)
-        twin_ready(3, 3)
-        project(3, 3)
-        finished(3)
-        q_outward(1)
-        landed(ext.at[halo_at(high)], er.at[2], z_in)
-
-    expand(1)
-    for pair in range(pairs):
-        windowed(pair)
-
-    def span(rel):
+        o_outer(2, 0)
+        for i in range(pairs):
+            att_landed(i)
+
+    def span(rel, first=0, count=out_chunks):
         h = g if rel == 0 else 1 - g
-        return pl.ds(pl.multiple_of(h * out_half, out_half), out_half)
+        return pl.ds(pl.multiple_of(h * out_half + first * out_size, out_size), count * out_size)
 
     def part_rows(dest):
         return pl.ds(pl.multiple_of(dest * share, share), share)
 
-    def emit(j, rel):
-        part[j, :, span(rel)] = jnp.dot(
-            att[...], wo[j, :, span(rel)], preferred_element_type=jnp.float32
-        ).astype(jnp.bfloat16)
-        for i in range(2):
-            exchange(j, rel, i)
-
-    def exchange(j, rel, i):
-        remote("both", lambda: (
-            part.at[j, part_rows(2 * i + 1 - core), span(rel)], dbuf.at[j, i, :, span(rel)],
-            ds.at[j, rel, i], dr.at[j, rel, i], {"tp": twin},
-        ))
-
-    def combine(j, rel):
-        for i in range(2):
-            landed(dbuf.at[j, i, :, span(rel)], dr.at[j, rel, i], {"tp": twin})
-        other = 1 - chip
-        both = (
-            part[j, part_rows(2 * other + core), span(rel)].astype(jnp.float32)
-            + dbuf[j, other, :, span(rel)].astype(jnp.float32)
-        )
-        xsend[j, :, span(rel)] = both.astype(jnp.bfloat16)
-        remote("both", lambda: (
-            xsend.at[j, :, span(rel)], xrecv.at[j, :, span(rel)], rxs.at[j, rel], rxr.at[j, rel], {"tp": across}
-        ))
-
-    def store(j, rel):
-        h = g if rel == 0 else 1 - g
-        at = pl.ds(pl.multiple_of(place_of(j) * out_cols + h * out_half, out_half), out_half)
-        return pltpu.make_async_copy(ostage.at[j, :, span(rel)], out_hbm.at[:, at], store_sem.at[j, rel])
-
-    def settle(j, rel):
-        landed(xrecv.at[j, :, span(rel)], rxr.at[j, rel], {"tp": across})
-        total = (
-            part[j, part_rows(t), span(rel)].astype(jnp.float32)
-            + dbuf[j, chip, :, span(rel)].astype(jnp.float32)
-            + xrecv[j, :, span(rel)].astype(jnp.float32)
-        )
-        ostage[j, :, span(rel)] = total.astype(jnp.bfloat16)
-        store(j, rel).start()
-
-    def arrive(j, rel):
-        if (j, rel) == (1, 1):
-
-            @pl.when(inner)
-            def _():
-                for c in all_out:
+    def tail(role, script):
+        def emit(j, rel, *cut):
+            lanes = span(rel, *cut)
+            part[j, :, lanes] = jnp.dot(
+                att[0], wo[j, :, lanes], preferred_element_type=jnp.float32
+            ).astype(jnp.bfloat16)
+            for i in range(2):
+                exchange(i, j, rel, *cut)
+
+        def exchange(i, j, rel, *cut):
+            at = cut[0] if cut else 0
+            remote(role, lambda: (
+                part.at[j, part_rows(2 * i + 1 - core), span(rel, *cut)], dbuf.at[j, i, :, span(rel, *cut)],
+                ds.at[j, rel, at, i], dr.at[j, rel, at, i], {"tp": twin},
+            ))
+
+        def combine(j, rel, *cut):
+            at = cut[0] if cut else 0
+            lanes = span(rel, *cut)
+            for i in range(2):
+                landed(dbuf.at[j, i, :, lanes], dr.at[j, rel, at, i], {"tp": twin})
+            other = 1 - chip
+            both = (
+                part[j, part_rows(2 * other + core), lanes].astype(jnp.float32)
+                + dbuf[j, other, :, lanes].astype(jnp.float32)
+            )
+            xsend[j, :, lanes] = both.astype(jnp.bfloat16)
+            remote(role, lambda: (
+                xsend.at[j, :, span(rel, *cut)], xrecv.at[j, :, span(rel, *cut)],
+                rxs.at[j, rel, at], rxr.at[j, rel, at], {"tp": across},
+            ))
+
+        stores = []
+
+        def settle(j, rel, *cut):
+            at = cut[0] if cut else 0
+            lanes = span(rel, *cut)
+            landed(xrecv.at[j, :, lanes], rxr.at[j, rel, at], {"tp": across})
+            total = (
+                part[j, part_rows(t), lanes].astype(jnp.float32)
+                + dbuf[j, chip, :, lanes].astype(jnp.float32)
+                + xrecv[j, :, lanes].astype(jnp.float32)
+            )
+            ostage[j, :, lanes] = total.astype(jnp.bfloat16)
+            first, count = cut if cut else (0, out_chunks)
+            h = g if rel == 0 else 1 - g
+            base = place_of(j) * out_cols + h * out_half + first * out_size
+            to = pl.ds(pl.multiple_of(base, out_size), count * out_size)
+            copy = pltpu.make_async_copy(ostage.at[j, :, lanes], out_hbm.at[:, to], store_sem.at[j, rel, at])
+            stores.append(copy)
+            copy.start()
+
+        def ready(j, first=0, count=out_chunks):
+            for c in range(first, first + count):
+                if role == "inner" and j == 1:
                     o_landed(1, 1, c, z_out)
-
-            @pl.when(outer)
-            def _():
-                for c in all_out:
-                    o_twin_landed(1, c)
-
-        elif rel == 1 and j > 1:
-            for c in all_out:
-                o_twin_landed(j, c)
-        elif (j, rel) == (3, 0):
-
-            @pl.when(inner)
-            def _():
-                for c in all_out:
-                    o_crossing(3, c)
-
-            @pl.when(outer)
-            def _():
-                for c in all_out:
-                    o_outer(3, c)
-
-    order = ((0, 0), (0, 1), (1, 0), (2, 0), (2, 1), (3, 0), (1, 1), (3, 1))
-    for i, piece in enumerate(order):
-        arrive(*piece)
-        emit(*piece)
-        if i >= 1:
-            combine(*order[i - 1])
-        if i >= 2:
-            settle(*order[i - 2])
-    combine(*order[-1])
-    settle(*order[-2])
-    settle(*order[-1])
+                else:
+                    o_twin_landed(j, c)
+
+        def pump(j, c):
+            if role == "inner":
+                o_crossing(j, c)
+            else:
+                o_outer(j, c)
+
+        words = {"emit": emit, "combine": combine, "settle": settle, "ready": ready, "pump": pump}
+        for word, *piece in script:
+            words[word](*piece)
+        for copy in stores:
+            copy.wait()
+
+    closing = [
+        ("settle", 0, 0), ("settle", 0, 1), ("settle", 1, 0), ("settle", 2, 0), ("settle", 2, 1),
+        ("settle", 3, 0, 0, 2), ("settle", 3, 0, 2, 2), ("settle", 3, 1, 0, 2),
+    ]
+    opening = [("emit", 0, 0), ("emit", 0, 1), ("combine", 0, 0), ("emit", 1, 0), ("combine", 0, 1)]
+    inner_script = (
+        opening
+        + [("pump", 3, 2), ("emit", 2, 0), ("combine", 1, 0), ("ready", 2), ("emit", 2, 1), ("combine", 2, 0)]
+        + [("pump", 3, 3), ("emit", 3, 0, 0, 2), ("combine", 2, 1), ("emit", 3, 0, 2, 2), ("combine", 3, 0, 0, 2)]
+        + [("ready", 1), ("emit", 1, 1), ("combine", 3, 0, 2, 2), ("ready", 3, 0, 2), ("emit", 3, 1, 0, 2)]
+        + [("combine", 1, 1), ("ready", 3, 2, 2), ("emit", 3, 1, 2, 2), ("combine", 3, 1, 0, 2)]
+        + [("combine", 3, 1, 2, 2)]
+        + closing + [("settle", 1, 1), ("settle", 3, 1, 2, 2)]
+    )
+    outer_script = (
+        opening
+        + [("pump", 2, 1), ("ready", 1), ("emit", 1, 1), ("combine", 1, 0), ("pump", 2, 2), ("combine", 1, 1)]
+        + [("pump", 2, 3), ("emit", 2, 0), ("pump", 3, 0), ("combine", 2, 0), ("ready", 2), ("emit", 2, 1)]
+        + [("pump", 3, 1), ("combine", 2, 1), ("pump", 3, 2), ("emit", 3, 0, 0, 2), ("pump", 3, 3)]
+        + [("combine", 3, 0, 0, 2), ("emit", 3, 0, 2, 2), ("ready", 3, 0, 2), ("emit", 3, 1, 0, 2)]
+        + [("combine", 3, 0, 2, 2), ("ready", 3, 2, 2), ("emit", 3, 1, 2, 2), ("combine", 3, 1, 0, 2)]
+        + [("combine", 3, 1, 2, 2)]
+        + closing[:4] + [("settle", 1, 1)] + closing[4:] + [("settle", 3, 1, 2, 2)]
+    )
+
+    @pl.when(inner)
+    def _():
+        tail("inner", inner_script)
+
+    @pl.when(outer)
+    def _():
+        tail("outer", outer_script)
 
     for role, test in (("inner", inner), ("outer", outer)):
 
@@ -1203,12 +1218,6 @@
             for when, build in sent:
                 if when == role:
                     build().wait_send()
-
-    for when, build in sent:
-        if when == "both":
-            build().wait_send()
-    for piece in order:
-        store(*piece).wait()
 
 
 def local(*args):
@@ -1252,21 +1261,18 @@
             pltpu.VMEM((2 * length, width), bf16),
             pltpu.VMEM((KINDS, n, depth, cols), bf16),
             pltpu.VMEM((n, out_rows, out_cols), bf16),
-            pltpu.VMEM((2 * length, cols), jnp.float32),
+            pltpu.VMEM((2, 2 * length, cols), jnp.float32),
             pltpu.VMEM((n, length, cols), bf16),
-            pltpu.VMEM((length + 2 * WINDOW, cols), bf16),
-            pltpu.VMEM((length, cols), bf16),
-            pltpu.VMEM((2, length, cols), bf16),
-            pltpu.VMEM((2, length, cols), bf16),
-            pltpu.VMEM((q_heads, length, LANES), bf16),
-            pltpu.VMEM((length, out_rows), bf16),
+            pltpu.VMEM((2, length + 2 * WINDOW, cols), bf16),
+            pltpu.VMEM((2, 2, q_heads, length, LANES), bf16),
+            pltpu.VMEM((2, length, out_rows), bf16),
             pltpu.VMEM((n, length, out_cols), bf16),
             pltpu.VMEM((n, 2, share, out_cols), bf16),
             pltpu.VMEM((n, share, out_cols), bf16),
             pltpu.VMEM((n, share, out_cols), bf16),
             pltpu.VMEM((n, share, out_cols), bf16),
             sem(9),
-            sem(n, HALVES),
+            sem(n, HALVES, out_chunks),
             sem(KINDS, 2, HALVES, chunks),
             sem(KINDS, n, HALVES, chunks),
             sem(KINDS, n, chunks),
@@ -1278,8 +1284,9 @@
             sem(n, out_chunks),
         ]
         + [sem(pieces)] * 8
-        + [sem(2), sem(n), sem(n), sem(3), sem(3), sem(2), sem(2)]
-        + [sem(n, HALVES, 2), sem(n, HALVES, 2), sem(n, HALVES), sem(n, HALVES)],
+        + [sem(2), sem(n), sem(1), sem(1), sem(q_heads), sem(q_heads)]
+        + [sem(n, HALVES, out_chunks, 2)] * 2
+        + [sem(n, HALVES, out_chunks)] * 2,
         compiler_params=pltpu.CompilerParams(
             collective_id=0, has_side_effects=True, vmem_limit_bytes=62 * 1024 * 1024
         ),

time: 135 us -> 111 us (0.82)
  Pallas kernels: 133 us -> 109 us
    pallas_call x1, Pallas kernels: 133 us -> 109 us  [local(): pl.pallas_call(functools.partial(pair_kernel, (q_heads, kv_heads)), out_s...]
where the time goes in v2:
time: 111 us
  Pallas kernels  109 us (98%)
  local copies, waits for them, and re-layouts  2.06 us (2%)
    pallas_call x1, Pallas kernels, local(): pl.pallas_call(functools.partial(pair_kernel, (q_heads, kv_heads)), out_s...  109 us

profile of v2, /device:TPU:0, one launch (start us, length us, event | category | flops | bytes accessed | tf_op | source)
XLA Modules:
  0.0 110.8 jit_solution(16418730895051094169)
XLA Ops:
  0.0 108.7 %shard_map.154 = bf16[96,4096]{1,0:T(8,128)(2,1)} custom-call(f32[1,4096]{1,0:T(1,128)} %bitcast.6, f32[4,128]{1,0:T(4,128)} %constant.2.clone.refs_1_, f32[1,64]{1,0:T(1,128)} %bitcast.7, f32[1,64]{1,0:T(1,128)} %bitcast.8, f32[1,64]{1,0:T(1,128)} %bitcast.9, f32[1,64]{1,0:T(1,128)} %bitcast.10, f32[1,4]{1,0:T(1,128)} %bitcast.11, ...), custom_call_target="tpu_custom_call" | custom-call | tf_op jit(solution)/shard_map/pallas_call | solution.py:1250
  108.7 2.1 %copy.18 = bf16[96,4096]{1,0:T(8,128)(2,1)} copy(bf16[96,4096]{1,0:T(8,128)(2,1)} %shard_map.154) | data formatting | bytes 1572864

commit v3 on v2

--- a/solution.py
+++ b/solution.py
@@ -599,6 +599,7 @@
 
 KINDS = 4
 SHARED = (True, False, False, False)
+RECEIVES, SENDS, LOCALS = 131, 109, 20
 
 def pair_kernel(sizes, *refs):
     gain_ref, fixed_ref, g0, g1, g2, g3, sink_ref, x_hbm = refs[:8]
@@ -608,11 +609,10 @@
 
 def run_pairs(
     sizes, gain_ref, fixed_ref, head_gains, sink_ref, x_hbm, weights, outs, out_hbm,
-    small_ref, tables_ref, xv, xn, wbuf, wo, proj, kvd, ext, qs, att, part, dbuf, xsend, xrecv, ostage,
-    load_sem, store_sem, zs, zr, ys, yr, wis, wzr, wos, wys, wyr,
-    xzs, xzr, xxs, xxr, xds, xdr, xes, xer, kis, kr, hs, hr, ats, atr, ds, dr, rxs, rxr,
+    small_ref, tables_ref, xv, xn, wbuf, wo, proj, kvd, ext, qs, att, part, dbuf, xsend, xrecv, ostage, mpart, mbuf, msum,
+    recv_sem, send_sem, load_sem,
 ):
-    q_heads, kv_heads = sizes
+    q_heads, kv_heads, chunks, out_chunks = sizes
     n, s = lax.axis_size("sp"), lax.axis_index("sp")
     n_tp, t = lax.axis_size("tp"), lax.axis_index("tp")
     g = lax.axis_index("grp")
@@ -620,7 +620,6 @@
     depth, cols = wbuf.shape[2], wbuf.shape[3]
     out_rows, out_cols = wo.shape[1], wo.shape[2]
     share = length // n_tp
-    chunks, out_chunks = zs.shape[3], wis.shape[2]
     low = 2 * s < n
     high = jnp.logical_not(low)
     inner = (s > 0) & (s < n - 1)
@@ -638,19 +637,30 @@
             return s
         return jnp.where(inner, (s - step, s - step, s + step, s + 2 * step)[j], s + j * step)
 
-    sent = []
-
-    def remote(when, ends):
+    sent = {"inner": [], "outer": []}
+    names = {}
+
+    def recv_at(*name):
+        at = names.setdefault(name, len(names))
+        assert at < recv_sem.shape[0]
+        return recv_sem.at[at]
+
+    def remote(when, name, ends):
+        at = len(sent[when])
+        assert at < send_sem.shape[0]
+
         def build():
-            src, dst, send, recv, peer = ends()
+            src, dst, peer = ends()
             return pltpu.make_async_remote_copy(
-                src_ref=src, dst_ref=dst, send_sem=send, recv_sem=recv, device_id=peer, device_id_type=MESH
+                src_ref=src, dst_ref=dst, send_sem=send_sem.at[at], recv_sem=recv_at(*name),
+                device_id=peer, device_id_type=MESH,
             )
 
-        sent.append((when, build))
+        sent[when].append(build)
         build().start()
 
-    def landed(ref, sem, peer):
+    def landed(ref, name, peer):
+        sem = recv_at(*name)
         pltpu.make_async_remote_copy(
             src_ref=ref, dst_ref=ref, send_sem=sem, recv_sem=sem, device_id=peer, device_id_type=MESH
         ).wait_recv()
@@ -666,20 +676,16 @@
 
     def w_inward(role, k, slot, rel, c):
         to = 1 if role == "outer" else slot + 2
-        remote(role, lambda: (
-            w_at(k, slot, rel, c), w_at(k, to, rel, c), zs.at[k, slot, rel, c], zr.at[k, to, rel, c], z_in
-        ))
+        remote(role, ("w", k, to, rel, c), lambda: (w_at(k, slot, rel, c), w_at(k, to, rel, c), z_in))
 
     def w_landed(k, slot, rel, c):
-        landed(w_at(k, slot, rel, c), zr.at[k, slot, rel, c], z_out if slot == 1 else z_in)
+        landed(w_at(k, slot, rel, c), ("w", k, slot, rel, c), z_out if slot == 1 else z_in)
 
     def w_twin(k, slot, c):
-        remote("inner", lambda: (
-            w_at(k, slot, 0, c), w_at(k, slot, 0, c), ys.at[k, slot, c], yr.at[k, slot, c], y_peer
-        ))
+        remote("inner", ("wy", k, slot, c), lambda: (w_at(k, slot, 0, c), w_at(k, slot, 0, c), y_peer))
 
     def w_twin_landed(k, slot, c):
-        landed(w_at(k, slot, 1, c), yr.at[k, slot, c], y_peer)
+        landed(w_at(k, slot, 1, c), ("wy", k, slot, c), y_peer)
 
     out_half = out_cols // HALVES
     out_size = out_half // out_chunks
@@ -690,24 +696,20 @@
 
     def o_inward(role, slot, rel, c):
         to = 1 if role == "outer" else slot + 2
-        remote(role, lambda: (
-            o_at(slot, rel, c), o_at(to, rel, c), wis.at[slot, rel, c], wzr.at[to, rel, c], z_in
-        ))
+        remote(role, ("o", to, rel, c), lambda: (o_at(slot, rel, c), o_at(to, rel, c), z_in))
 
     def o_outward(slot, c):
         to = 1 if slot == 0 else slot
-        remote("inner", lambda: (
-            o_at(slot, 0, c), o_at(to, 0, c), wos.at[slot, c], wzr.at[to, 0, c], z_out
-        ))
+        remote("inner", ("o", to, 0, c), lambda: (o_at(slot, 0, c), o_at(to, 0, c), z_out))
 
     def o_landed(slot, rel, c, peer):
-        landed(o_at(slot, rel, c), wzr.at[slot, rel, c], peer)
+        landed(o_at(slot, rel, c), ("o", slot, rel, c), peer)
 
     def o_twin(role, slot, c):
-        remote(role, lambda: (o_at(slot, 0, c), o_at(slot, 0, c), wys.at[slot, c], wyr.at[slot, c], y_peer))
+        remote(role, ("oy", slot, c), lambda: (o_at(slot, 0, c), o_at(slot, 0, c), y_peer))
 
     def o_twin_landed(slot, c):
-        landed(o_at(slot, 1, c), wyr.at[slot, c], y_peer)
+        landed(o_at(slot, 1, c), ("oy", slot, c), y_peer)
 
     def x_rows(quarter):
         return pl.ds(pl.multiple_of(length + quarter * share, share), share)
@@ -719,20 +721,20 @@
         def piece():
             return xn.at[x_rows(t), x_cols(p)]
 
-        landed(piece(), xzr.at[p], z_out)
-        remote("inner", lambda: (piece(), piece(), xxs.at[p], xxr.at[p], {"tp": across}))
-        remote("inner", lambda: (piece(), piece(), xds.at[p], xdr.at[p], {"tp": twin}))
+        landed(piece(), ("x", p), z_out)
+        remote("inner", ("xx", p), lambda: (piece(), piece(), {"tp": across}))
+        remote("inner", ("xd", p), lambda: (piece(), piece(), {"tp": twin}))
 
     def x_pass(p):
         def piece():
             return xn.at[x_rows(across), x_cols(p)]
 
-        landed(piece(), xxr.at[p], {"tp": across})
-        remote("inner", lambda: (piece(), piece(), xes.at[p], xer.at[p], {"tp": twin}))
+        landed(piece(), ("xx", p), {"tp": across})
+        remote("inner", ("xe", p), lambda: (piece(), piece(), {"tp": twin}))
 
     def x_all(p):
-        landed(xn.at[x_rows(twin), x_cols(p)], xdr.at[p], {"tp": twin})
-        landed(xn.at[x_rows(diagonal), x_cols(p)], xer.at[p], {"tp": twin})
+        landed(xn.at[x_rows(twin), x_cols(p)], ("xd", p), {"tp": twin})
+        landed(xn.at[x_rows(diagonal), x_cols(p)], ("xe", p), {"tp": twin})
 
     kv_cols = cols // 2
     loads = []
@@ -863,7 +865,8 @@
 
     def o_crossing(slot, c):
         o_landed(slot, 0, c, z_in)
-        o_outward(slot, c)
+        if slot < 3:
+            o_outward(slot, c)
         o_twin("inner", slot, c)
 
     def o_outer(slot, c):
@@ -877,10 +880,10 @@
         return pl.ds(jnp.where(leading, 0, WINDOW + length), WINDOW)
 
     def halo_inward():
-        remote("inner", lambda: (ext.at[0, edge(high)], ext.at[0, halo_at(low)], hs.at[0], hr.at[0], z_in))
+        remote("inner", ("halo",), lambda: (ext.at[0, edge(high)], ext.at[0, halo_at(low)], z_in))
 
     def halo_landed():
-        landed(ext.at[0, halo_at(high)], hr.at[0], z_in)
+        landed(ext.at[0, halo_at(high)], ("halo",), z_in)
 
     def halo_local():
         ext[0, halo_at(low), :] = ext[1, edge(high), :]
@@ -888,24 +891,22 @@
         ext[1, halo_at(low), :] = jnp.zeros((WINDOW, cols), jnp.bfloat16)
 
     def kv_landed(j):
-        landed(kvd.at[j], kr.at[j], z_in)
+        landed(kvd.at[j], ("kv", j), z_in)
 
     def kv_inward(j):
-        remote("inner", lambda: (kvd.at[j], kvd.at[j + 2], kis.at[j], kr.at[j + 2], z_in))
+        remote("inner", ("kv", j + 2), lambda: (kvd.at[j], kvd.at[j + 2], z_in))
 
     def x_inward(p):
-        remote("outer", lambda: (
-            xn.at[0:share, x_cols(p)], xn.at[x_rows(t), x_cols(p)], xzs.at[p], xzr.at[p], z_in
-        ))
+        remote("outer", ("x", p), lambda: (xn.at[0:share, x_cols(p)], xn.at[x_rows(t), x_cols(p)], z_in))
 
     def att_at(side, i):
         return att.at[side, :, i * LANES : (i + 1) * LANES]
 
     def att_outward(i):
-        remote("inner", lambda: (att_at(1, i), att_at(0, i), ats.at[i], atr.at[i], z_out))
+        remote("inner", ("att", i), lambda: (att_at(1, i), att_at(0, i), z_out))
 
     def att_landed(i):
-        landed(att_at(0, i), atr.at[i], z_in)
+        landed(att_at(0, i), ("att", i), z_in)
 
     def joined(results, pair):
         side = (kv_heads + pair * 2 // group) % 2
@@ -1050,20 +1051,23 @@
         att_outward(pairs)
         crossing(2, 3, 1)
         mates(3, 1)
-        for c in all_out:
+        for c in range(2):
             o_inward("inner", 0, 0, c)
         dense(1, 1)
         att_outward(pairs + 1)
+        crossing(3, 3, 0)
+        dense(0, 0)
         mate_ready(2)
-        crossing(3, 3, 0)
         project(2, 1)
+        crossing(3, 3, 1)
         twin_ready(2, 3)
         project(2, 3)
         project(3, 0)
-        crossing(3, 3, 1)
         finished(2, 1)
         finished(2, 0)
         halo_inward()
+        for c in range(2, out_chunks):
+            o_inward("inner", 0, 0, c)
         halo_local()
         twin_ready(3, 2)
         project(3, 2)
@@ -1073,26 +1077,24 @@
         twin_ready(3, 3)
         project(3, 3, (1,))
         finished(3, 1)
-        o_mates(0)
         windowed(1, 0)
         att_outward(0)
         windowed(1, 1)
         att_outward(1)
         o_crossing(2, 1)
-        o_mates(1)
+        o_mates(0)
         project(3, 3, (0,))
         finished(3, 0)
         halo_landed()
+        o_mates(1)
+        windowed(0, 0)
         o_crossing(2, 2)
+        windowed(0, 1)
         o_mates(2)
-        windowed(0, 0)
-        windowed(0, 1)
+        dense(0, 1)
         o_crossing(2, 3)
         o_mates(3)
-        dense(0, 0)
         o_crossing(3, 0)
-        dense(0, 1)
-        o_crossing(3, 1)
 
     @pl.when(outer)
     def _():
@@ -1104,58 +1106,67 @@
         h = g if rel == 0 else 1 - g
         return pl.ds(pl.multiple_of(h * out_half + first * out_size, out_size), count * out_size)
 
-    def part_rows(dest):
-        return pl.ds(pl.multiple_of(dest * share, share), share)
-
     def tail(role, script):
-        def emit(j, rel, *cut):
-            lanes = span(rel, *cut)
-            part[j, :, lanes] = jnp.dot(
-                att[0], wo[j, :, lanes], preferred_element_type=jnp.float32
-            ).astype(jnp.bfloat16)
-            for i in range(2):
-                exchange(i, j, rel, *cut)
-
-        def exchange(i, j, rel, *cut):
-            at = cut[0] if cut else 0
-            remote(role, lambda: (
-                part.at[j, part_rows(2 * i + 1 - core), span(rel, *cut)], dbuf.at[j, i, :, span(rel, *cut)],
-                ds.at[j, rel, at, i], dr.at[j, rel, at, i], {"tp": twin},
+        def emit(*piece):
+            j, lanes = piece[0], span(*piece[1:])
+            found = jnp.dot(att[0], wo[j, :, lanes], preferred_element_type=jnp.float32).astype(jnp.bfloat16)
+            for dest in range(n_tp):
+                part[j, dest % 2, dest // 2, :, lanes] = found[dest * share : (dest + 1) * share]
+            remote(role, ("d",) + piece, lambda: (
+                part.at[j, 1 - core, :, :, span(*piece[1:])], dbuf.at[j, :, :, span(*piece[1:])], {"tp": twin}
             ))
 
-        def combine(j, rel, *cut):
-            at = cut[0] if cut else 0
-            lanes = span(rel, *cut)
-            for i in range(2):
-                landed(dbuf.at[j, i, :, lanes], dr.at[j, rel, at, i], {"tp": twin})
-            other = 1 - chip
+        def combine(*piece):
+            j, lanes = piece[0], span(*piece[1:])
+            landed(dbuf.at[j, :, :, lanes], ("d",) + piece, {"tp": twin})
             both = (
-                part[j, part_rows(2 * other + core), lanes].astype(jnp.float32)
-                + dbuf[j, other, :, lanes].astype(jnp.float32)
+                part[j, core, 1 - chip, :, lanes].astype(jnp.float32) + dbuf[j, 1 - chip, :, lanes].astype(jnp.float32)
             )
             xsend[j, :, lanes] = both.astype(jnp.bfloat16)
-            remote(role, lambda: (
-                xsend.at[j, :, span(rel, *cut)], xrecv.at[j, :, span(rel, *cut)],
-                rxs.at[j, rel, at], rxr.at[j, rel, at], {"tp": across},
+            remote(role, ("r",) + piece, lambda: (
+                xsend.at[j, :, span(*piece[1:])], xrecv.at[j, :, span(*piece[1:])], {"tp": across}
             ))
 
+        def emit_mate(*piece):
+            j, lanes = piece[0], span(*piece[1:])
+            found = jnp.dot(att[1], wo[j, :, lanes], preferred_element_type=jnp.float32).astype(jnp.bfloat16)
+            for dest in range(n_tp):
+                mpart[dest % 2, dest // 2, :, lanes] = found[dest * share : (dest + 1) * share]
+            remote(role, ("md",) + piece, lambda: (
+                mpart.at[1 - core, :, :, span(*piece[1:])], mbuf.at[:, :, span(*piece[1:])], {"tp": twin}
+            ))
+
+        def combine_mate(*piece):
+            lanes = span(*piece[1:])
+            landed(mbuf.at[:, :, lanes], ("md",) + piece, {"tp": twin})
+            both = mpart[core, :, :, lanes].astype(jnp.float32) + mbuf[:, :, lanes].astype(jnp.float32)
+            msum[:, :, lanes] = both.astype(jnp.bfloat16)
+            remote(role, ("m",) + piece, lambda: (
+                msum.at[:, :, span(*piece[1:])], msum.at[:, :, span(*piece[1:])], z_out
+            ))
+
+        def relay(*piece):
+            landed(msum.at[:, :, span(*piece[1:])], ("m",) + piece, z_in)
+            remote(role, ("r",) + piece, lambda: (
+                msum.at[1 - chip, :, span(*piece[1:])], xrecv.at[piece[0], :, span(*piece[1:])], {"tp": across}
+            ))
+
         stores = []
 
-        def settle(j, rel, *cut):
-            at = cut[0] if cut else 0
-            lanes = span(rel, *cut)
-            landed(xrecv.at[j, :, lanes], rxr.at[j, rel, at], {"tp": across})
-            total = (
-                part[j, part_rows(t), lanes].astype(jnp.float32)
-                + dbuf[j, chip, :, lanes].astype(jnp.float32)
-                + xrecv[j, :, lanes].astype(jnp.float32)
-            )
+        def settle(*piece):
+            j, lanes = piece[0], span(*piece[1:])
+            landed(xrecv.at[j, :, lanes], ("r",) + piece, {"tp": across})
+            if role == "outer" and j == 3:
+                near = msum[chip, :, lanes].astype(jnp.float32)
+            else:
+                near = part[j, core, chip, :, lanes].astype(jnp.float32) + dbuf[j, chip, :, lanes].astype(jnp.float32)
+            total = near + xrecv[j, :, lanes].astype(jnp.float32)
             ostage[j, :, lanes] = total.astype(jnp.bfloat16)
-            first, count = cut if cut else (0, out_chunks)
+            rel, first, count = piece[1:] if len(piece) > 2 else (piece[1], 0, out_chunks)
             h = g if rel == 0 else 1 - g
             base = place_of(j) * out_cols + h * out_half + first * out_size
             to = pl.ds(pl.multiple_of(base, out_size), count * out_size)
-            copy = pltpu.make_async_copy(ostage.at[j, :, lanes], out_hbm.at[:, to], store_sem.at[j, rel, at])
+            copy = pltpu.make_async_copy(ostage.at[j, :, lanes], out_hbm.at[:, to], load_sem.at[len(loads) + len(stores)])
             stores.append(copy)
             copy.start()
 
@@ -1172,35 +1183,41 @@
             else:
                 o_outer(j, c)
 
-        words = {"emit": emit, "combine": combine, "settle": settle, "ready": ready, "pump": pump}
+        words = {
+            "emit": emit, "combine": combine, "settle": settle, "ready": ready, "pump": pump,
+            "emit_mate": emit_mate, "combine_mate": combine_mate, "relay": relay,
+        }
         for word, *piece in script:
             words[word](*piece)
         for copy in stores:
             copy.wait()
 
-    closing = [
-        ("settle", 0, 0), ("settle", 0, 1), ("settle", 1, 0), ("settle", 2, 0), ("settle", 2, 1),
-        ("settle", 3, 0, 0, 2), ("settle", 3, 0, 2, 2), ("settle", 3, 1, 0, 2),
-    ]
     opening = [("emit", 0, 0), ("emit", 0, 1), ("combine", 0, 0), ("emit", 1, 0), ("combine", 0, 1)]
+    last = [(3, 1, 0, 2), (3, 1, 2, 1), (3, 1, 3, 1)]
+    far = [(3, 0, 0, 2), (3, 0, 2, 2)] + last
     inner_script = (
         opening
-        + [("pump", 3, 2), ("emit", 2, 0), ("combine", 1, 0), ("ready", 2), ("emit", 2, 1), ("combine", 2, 0)]
-        + [("pump", 3, 3), ("emit", 3, 0, 0, 2), ("combine", 2, 1), ("emit", 3, 0, 2, 2), ("combine", 3, 0, 0, 2)]
-        + [("ready", 1), ("emit", 1, 1), ("combine", 3, 0, 2, 2), ("ready", 3, 0, 2), ("emit", 3, 1, 0, 2)]
-        + [("combine", 1, 1), ("ready", 3, 2, 2), ("emit", 3, 1, 2, 2), ("combine", 3, 1, 0, 2)]
-        + [("combine", 3, 1, 2, 2)]
-        + closing + [("settle", 1, 1), ("settle", 3, 1, 2, 2)]
+        + [("emit", 2, 0), ("combine", 1, 0), ("pump", 3, 1), ("ready", 2), ("emit", 2, 1), ("combine", 2, 0)]
+        + [("pump", 3, 2), ("combine", 2, 1), ("emit_mate",) + far[0], ("emit",) + far[0]]
+        + [("pump", 3, 3), ("combine_mate",) + far[0], ("emit_mate",) + far[1], ("emit",) + far[1]]
+        + [("combine",) + far[0], ("ready", 3, 0, 2), ("combine_mate",) + far[1], ("emit_mate",) + last[0]]
+        + [("emit",) + last[0], ("combine",) + far[1], ("ready", 1), ("emit", 1, 1)]
+        + [("combine_mate",) + last[0], ("combine",) + last[0], ("combine", 1, 1)]
+        + [("ready", 3, 2, 1), ("emit_mate",) + last[1], ("emit",) + last[1]]
+        + [("settle", 0, 0), ("settle", 0, 1), ("combine_mate",) + last[1]]
+        + [("ready", 3, 3, 1), ("emit_mate",) + last[2], ("emit",) + last[2]]
+        + [("combine",) + last[1], ("settle", 1, 0), ("combine_mate",) + last[2], ("combine",) + last[2]]
+        + [("settle", 2, 0), ("settle", 2, 1), ("settle",) + far[0], ("settle",) + far[1]]
+        + [("settle",) + last[0], ("settle", 1, 1)] + [("settle",) + piece for piece in last[1:]]
     )
     outer_script = (
         opening
         + [("pump", 2, 1), ("ready", 1), ("emit", 1, 1), ("combine", 1, 0), ("pump", 2, 2), ("combine", 1, 1)]
-        + [("pump", 2, 3), ("emit", 2, 0), ("pump", 3, 0), ("combine", 2, 0), ("ready", 2), ("emit", 2, 1)]
-        + [("pump", 3, 1), ("combine", 2, 1), ("pump", 3, 2), ("emit", 3, 0, 0, 2), ("pump", 3, 3)]
-        + [("combine", 3, 0, 0, 2), ("emit", 3, 0, 2, 2), ("ready", 3, 0, 2), ("emit", 3, 1, 0, 2)]
-        + [("combine", 3, 0, 2, 2), ("ready", 3, 2, 2), ("emit", 3, 1, 2, 2), ("combine", 3, 1, 0, 2)]
-        + [("combine", 3, 1, 2, 2)]
-        + closing[:4] + [("settle", 1, 1)] + closing[4:] + [("settle", 3, 1, 2, 2)]
+        + [("pump", 2, 3), ("emit", 2, 0), ("ready", 2, 0, 2), ("combine", 2, 0)]
+        + [("ready", 2, 2, 2), ("emit", 2, 1), ("settle", 0, 0), ("relay",) + far[0], ("combine", 2, 1)]
+        + [("settle", 0, 1), ("settle", 1, 0), ("relay",) + far[1], ("settle", 1, 1), ("relay",) + last[0]]
+        + [("settle", 2, 0), ("relay",) + last[1], ("relay",) + last[2], ("settle", 2, 1)]
+        + [("settle",) + piece for piece in far]
     )
 
     @pl.when(inner)
@@ -1215,9 +1232,8 @@
 
         @pl.when(test)
         def _():
-            for when, build in sent:
-                if when == role:
-                    build().wait_send()
+            for build in sent[role]:
+                build().wait_send()
 
 
 def local(*args):
@@ -1240,7 +1256,7 @@
         + [np.where(lane % wide < wide // 2, -1.0, 1.0) for wide in (HD, HD // 2)]
     ).astype(np.float32)
     gains = [gain[None, :] for gain in (wq_gain, wk_gain, dq_gain, dk_gain)]
-    chunks, out_chunks, pieces = 2, 4, width // depth
+    chunks, out_chunks = 2, 4
     vmem = pl.BlockSpec(memory_space=pltpu.VMEM)
     bf16 = jnp.bfloat16
 
@@ -1248,7 +1264,7 @@
         return pltpu.SemaphoreType.DMA(shape)
 
     return pl.pallas_call(
-        functools.partial(pair_kernel, (q_heads, kv_heads)),
+        functools.partial(pair_kernel, (q_heads, kv_heads, chunks, out_chunks)),
         out_shape=jax.ShapeDtypeStruct((share, width), bf16),
         in_specs=[vmem] * 6
         + [pl.BlockSpec(memory_space=pltpu.SMEM)]
@@ -1266,27 +1282,18 @@
             pltpu.VMEM((2, length + 2 * WINDOW, cols), bf16),
             pltpu.VMEM((2, 2, q_heads, length, LANES), bf16),
             pltpu.VMEM((2, length, out_rows), bf16),
-            pltpu.VMEM((n, length, out_cols), bf16),
+            pltpu.VMEM((n, 2, n_tp // 2, share, out_cols), bf16),
             pltpu.VMEM((n, 2, share, out_cols), bf16),
             pltpu.VMEM((n, share, out_cols), bf16),
             pltpu.VMEM((n, share, out_cols), bf16),
             pltpu.VMEM((n, share, out_cols), bf16),
-            sem(9),
-            sem(n, HALVES, out_chunks),
-            sem(KINDS, 2, HALVES, chunks),
-            sem(KINDS, n, HALVES, chunks),
-            sem(KINDS, n, chunks),
-            sem(KINDS, n, chunks),
-            sem(2, HALVES, out_chunks),
-            sem(n, HALVES, out_chunks),
-            sem(n, out_chunks),
-            sem(n, out_chunks),
-            sem(n, out_chunks),
-        ]
-        + [sem(pieces)] * 8
-        + [sem(2), sem(n), sem(1), sem(1), sem(q_heads), sem(q_heads)]
-        + [sem(n, HALVES, out_chunks, 2)] * 2
-        + [sem(n, HALVES, out_chunks)] * 2,
+            pltpu.VMEM((2, n_tp // 2, share, out_cols), bf16),
+            pltpu.VMEM((n_tp // 2, share, out_cols), bf16),
+            pltpu.VMEM((n_tp // 2, share, out_cols), bf16),
+            sem(RECEIVES),
+            sem(SENDS),
+            sem(LOCALS),
+        ],
         compiler_params=pltpu.CompilerParams(
             collective_id=0, has_side_effects=True, vmem_limit_bytes=62 * 1024 * 1024
         ),

time: 111 us -> 103 us (0.928)
  Pallas kernels: 109 us -> 101 us
    pallas_call x1, Pallas kernels: 109 us -> 101 us  [local(): pl.pallas_call(functools.partial(pair_kernel, (q_heads, kv_heads, chunks,...]
where the time goes in v3:
time: 103 us
  Pallas kernels  101 us (98%)
  local copies, waits for them, and re-layouts  2.06 us (2%)
    pallas_call x1, Pallas kernels, local(): pl.pallas_call(functools.partial(pair_kernel, (q_heads, kv_heads, chunks,...  101 us
    unnamed x1, local copies, waits for them, and re-layouts  2.06 us

profile of v3, /device:TPU:0, one launch (start us, length us, event | category | flops | bytes accessed | tf_op | source)
XLA Modules:
  0.0 103.0 jit_solution(742967564117708832)
XLA Ops:
  0.0 100.9 %shard_map.154 = bf16[96,4096]{1,0:T(8,128)(2,1)} custom-call(f32[1,4096]{1,0:T(1,128)} %bitcast.6, f32[4,128]{1,0:T(4,128)} %constant.2.clone.refs_1_, f32[1,64]{1,0:T(1,128)} %bitcast.7, f32[1,64]{1,0:T(1,128)} %bitcast.8, f32[1,64]{1,0:T(1,128)} %bitcast.9, f32[1,64]{1,0:T(1,128)} %bitcast.10, f32[1,4]{1,0:T(1,128)} %bitcast.11, ...), custom_call_target="tpu_custom_call" | custom-call | tf_op jit(solution)/shard_map/pallas_call | solution.py:1266
  100.9 2.1 %copy.18 = bf16[96,4096]{1,0:T(8,128)(2,1)} copy(bf16[96,4096]{1,0:T(8,128)(2,1)} %shard_map.154) | data formatting | bytes 1572864

commit v4 on v3

--- a/solution.py
+++ b/solution.py
@@ -599,17 +599,17 @@
 
 KINDS = 4
 SHARED = (True, False, False, False)
-RECEIVES, SENDS, LOCALS = 131, 109, 20
+RECEIVES, SENDS, LOCALS = 131, 16, 9
 
 def pair_kernel(sizes, *refs):
     gain_ref, fixed_ref, g0, g1, g2, g3, sink_ref, x_hbm = refs[:8]
-    weights, outs, out_hbm = refs[8:14], refs[14:16], refs[16]
-    run_pairs(sizes, gain_ref, fixed_ref, (g0, g1, g2, g3), sink_ref, x_hbm, weights, outs, out_hbm, *refs[17:])
+    weights, outs, out_ref = refs[8:14], refs[14:16], refs[16]
+    run_pairs(sizes, gain_ref, fixed_ref, (g0, g1, g2, g3), sink_ref, x_hbm, weights, outs, out_ref, *refs[17:])
 
 
 def run_pairs(
-    sizes, gain_ref, fixed_ref, head_gains, sink_ref, x_hbm, weights, outs, out_hbm,
-    small_ref, tables_ref, xv, xn, wbuf, wo, proj, kvd, ext, qs, att, part, dbuf, xsend, xrecv, ostage, mpart, mbuf, msum,
+    sizes, gain_ref, fixed_ref, head_gains, sink_ref, x_hbm, weights, outs, out_ref,
+    small_ref, tables_ref, xv, xn, wbuf, wo, proj, kvd, ext, qs, att, part, dbuf, xsend, xrecv, mpart, mbuf, msum,
     recv_sem, send_sem, load_sem,
 ):
     q_heads, kv_heads, chunks, out_chunks = sizes
@@ -637,7 +637,7 @@
             return s
         return jnp.where(inner, (s - step, s - step, s + step, s + 2 * step)[j], s + j * step)
 
-    sent = {"inner": [], "outer": []}
+    sent = {"inner": {}, "outer": {}}
     names = {}
 
     def recv_at(*name):
@@ -645,19 +645,36 @@
         assert at < recv_sem.shape[0]
         return recv_sem.at[at]
 
-    def remote(when, name, ends):
-        at = len(sent[when])
+    def whole(when, group):
+        many = when == "inner"
+        return {
+            "w": lambda: wbuf.at[0] if many else wbuf.at[1:KINDS, 0],
+            "w0": lambda: wbuf.at[0, 0, 0:half],
+            "wy": lambda: wbuf.at[0],
+            "o": lambda: wo.at[0],
+            "oo": lambda: wo.at[0],
+            "oy": lambda: wo.at[0],
+            "x": lambda: xn.at[0:share],
+            "xx": lambda: xn.at[0:share],
+            "xd": lambda: xn.at[0:share],
+            "xe": lambda: xn.at[0:share],
+            "kv": lambda: kvd.at[0:2],
+            "halo": lambda: ext.at[0, 0:WINDOW],
+            "att": lambda: att.at[0],
+            "d": lambda: dbuf if many else dbuf.at[0:3],
+            "r": lambda: xrecv,
+            "md": lambda: mbuf,
+            "m": lambda: msum,
+        }[group]()
+
+    def remote(when, name, ends, group=None):
+        at = sent[when].setdefault(group or name[0], len(sent[when]))
         assert at < send_sem.shape[0]
-
-        def build():
-            src, dst, peer = ends()
-            return pltpu.make_async_remote_copy(
-                src_ref=src, dst_ref=dst, send_sem=send_sem.at[at], recv_sem=recv_at(*name),
-                device_id=peer, device_id_type=MESH,
-            )
-
-        sent[when].append(build)
-        build().start()
+        src, dst, peer = ends()
+        pltpu.make_async_remote_copy(
+            src_ref=src, dst_ref=dst, send_sem=send_sem.at[at], recv_sem=recv_at(*name),
+            device_id=peer, device_id_type=MESH,
+        ).start()
 
     def landed(ref, name, peer):
         sem = recv_at(*name)
@@ -676,13 +693,19 @@
 
     def w_inward(role, k, slot, rel, c):
         to = 1 if role == "outer" else slot + 2
-        remote(role, ("w", k, to, rel, c), lambda: (w_at(k, slot, rel, c), w_at(k, to, rel, c), z_in))
+        remote(
+            role, ("w", k, to, rel, c), lambda: (w_at(k, slot, rel, c), w_at(k, to, rel, c), z_in),
+            "w0" if role == "outer" and k == 0 else "w",
+        )
 
     def w_landed(k, slot, rel, c):
         landed(w_at(k, slot, rel, c), ("w", k, slot, rel, c), z_out if slot == 1 else z_in)
 
     def w_twin(k, slot, c):
-        remote("inner", ("wy", k, slot, c), lambda: (w_at(k, slot, 0, c), w_at(k, slot, 0, c), y_peer))
+        remote(
+            "inner", ("wy", k, slot, c), lambda: (w_at(k, slot, 0, c), w_at(k, slot, 0, c), y_peer),
+            "w0" if slot == 1 else "wy",
+        )
 
     def w_twin_landed(k, slot, c):
         landed(w_at(k, slot, 1, c), ("wy", k, slot, c), y_peer)
@@ -700,7 +723,7 @@
 
     def o_outward(slot, c):
         to = 1 if slot == 0 else slot
-        remote("inner", ("o", to, 0, c), lambda: (o_at(slot, 0, c), o_at(to, 0, c), z_out))
+        remote("inner", ("o", to, 0, c), lambda: (o_at(slot, 0, c), o_at(to, 0, c), z_out), "oo")
 
     def o_landed(slot, rel, c, peer):
         landed(o_at(slot, rel, c), ("o", slot, rel, c), peer)
@@ -1151,8 +1174,6 @@
                 msum.at[1 - chip, :, span(*piece[1:])], xrecv.at[piece[0], :, span(*piece[1:])], {"tp": across}
             ))
 
-        stores = []
-
         def settle(*piece):
             j, lanes = piece[0], span(*piece[1:])
             landed(xrecv.at[j, :, lanes], ("r",) + piece, {"tp": across})
@@ -1161,14 +1182,10 @@
             else:
                 near = part[j, core, chip, :, lanes].astype(jnp.float32) + dbuf[j, chip, :, lanes].astype(jnp.float32)
             total = near + xrecv[j, :, lanes].astype(jnp.float32)
-            ostage[j, :, lanes] = total.astype(jnp.bfloat16)
             rel, first, count = piece[1:] if len(piece) > 2 else (piece[1], 0, out_chunks)
             h = g if rel == 0 else 1 - g
             base = place_of(j) * out_cols + h * out_half + first * out_size
-            to = pl.ds(pl.multiple_of(base, out_size), count * out_size)
-            copy = pltpu.make_async_copy(ostage.at[j, :, lanes], out_hbm.at[:, to], load_sem.at[len(loads) + len(stores)])
-            stores.append(copy)
-            copy.start()
+            out_ref[:, pl.ds(pl.multiple_of(base, out_size), count * out_size)] = total.astype(jnp.bfloat16)
 
         def ready(j, first=0, count=out_chunks):
             for c in range(first, first + count):
@@ -1189,8 +1206,6 @@
         }
         for word, *piece in script:
             words[word](*piece)
-        for copy in stores:
-            copy.wait()
 
     opening = [("emit", 0, 0), ("emit", 0, 1), ("combine", 0, 0), ("emit", 1, 0), ("combine", 0, 1)]
     last = [(3, 1, 0, 2), (3, 1, 2, 1), (3, 1, 3, 1)]
@@ -1232,8 +1247,12 @@
 
         @pl.when(test)
         def _():
-            for build in sent[role]:
-                build().wait_send()
+            for group, at in sent[role].items():
+                ref = whole(role, group)
+                pltpu.make_async_remote_copy(
+                    src_ref=ref, dst_ref=ref, send_sem=send_sem.at[at], recv_sem=recv_sem.at[0],
+                    device_id=y_peer, device_id_type=MESH,
+                ).wait_send()
 
 
 def local(*args):
@@ -1265,11 +1284,11 @@
 
     return pl.pallas_call(
         functools.partial(pair_kernel, (q_heads, kv_heads, chunks, out_chunks)),
-        out_shape=jax.ShapeDtypeStruct((share, width), bf16),
+        out_shape=pltpu.VMEM((share, width), bf16),
         in_specs=[vmem] * 6
         + [pl.BlockSpec(memory_space=pltpu.SMEM)]
         + [pl.BlockSpec(memory_space=pl.ANY)] * 9,
-        out_specs=pl.BlockSpec(memory_space=pl.ANY),
+        out_specs=vmem,
         scratch_shapes=[
             pltpu.VMEM((8, LANES), jnp.float32),
             pltpu.VMEM((4, 2 * length, LANES), jnp.float32),
@@ -1284,7 +1303,6 @@
             pltpu.VMEM((2, length, out_rows), bf16),
             pltpu.VMEM((n, 2, n_tp // 2, share, out_cols), bf16),
             pltpu.VMEM((n, 2, share, out_cols), bf16),
-            pltpu.VMEM((n, share, out_cols), bf16),
             pltpu.VMEM((n, share, out_cols), bf16),
             pltpu.VMEM((n, share, out_cols), bf16),
             pltpu.VMEM((2, n_tp // 2, share, out_cols), bf16),

time: 103 us -> 100 us (0.971)
  Pallas kernels: 101 us -> 99.3 us
  local copies, waits for them, and re-layouts: 2.06 us -> 0.88 us
    pallas_call x1, Pallas kernels: 101 us -> 99.3 us  [local(): pl.pallas_call(functools.partial(pair_kernel, (q_heads, kv_heads, chunks,...]
    unnamed x1, local copies, waits for them, and re-layouts: 2.06 us -> 0.88 us
where the time goes in v4:
time: 100 us
  Pallas kernels  99.3 us (99%)
    pallas_call x1, Pallas kernels, local(): pl.pallas_call(functools.partial(pair_kernel, (q_heads, kv_heads, chunks,...  99.3 us

profile of v4, /device:TPU:0, one launch (start us, length us, event | category | flops | bytes accessed | tf_op | source)
XLA Modules:
  0.0 100.2 jit_solution(3662462180694358684)
XLA Ops:
  0.0 99.3 %shard_map.154 = bf16[96,4096]{1,0:T(8,128)(2,1)S(1)} custom-call(f32[1,4096]{1,0:T(1,128)} %bitcast.6, f32[4,128]{1,0:T(4,128)} %constant.2.clone.refs_1_, f32[1,64]{1,0:T(1,128)} %bitcast.7, f32[1,64]{1,0:T(1,128)} %bitcast.8, f32[1,64]{1,0:T(1,128)} %bitcast.9, f32[1,64]{1,0:T(1,128)} %bitcast.10, f32[1,4]{1,0:T(1,128)} %bitcast.11, ...), custom_call_target="tpu_custom_call" | custom-call | tf_op jit(solution)/shard_map/pallas_call | solution.py:1285
  99.3 0.9 copy.18

commit v5 on v4

--- a/solution.py
+++ b/solution.py
@@ -662,7 +662,7 @@
             "halo": lambda: ext.at[0, 0:WINDOW],
             "att": lambda: att.at[0],
             "d": lambda: dbuf if many else dbuf.at[0:3],
-            "r": lambda: xrecv,
+            "r": lambda: xrecv if many else xrecv.at[0:3],
             "md": lambda: mbuf,
             "m": lambda: msum,
         }[group]()
@@ -971,8 +971,8 @@
             found = jnp.dot(weight, value, preferred_element_type=jnp.float32)
             att[side, rows[b], pair * LANES : (pair + 1) * LANES] = joined((found[:WINDOW], found[WINDOW:]), pair)
 
-    def dense(side, pair):
-        @pl.loop(0, length // LANES)
+    def dense(side, pair, first=0, last=length // LANES):
+        @pl.loop(first, last)
         def _(b):
             rows = pl.ds(pl.multiple_of(b * LANES, LANES), LANES)
             key = kvd[:, :, tile_of(2 * pair // group)].reshape(total_len, LANES)
@@ -1114,10 +1114,11 @@
         o_crossing(2, 2)
         windowed(0, 1)
         o_mates(2)
-        dense(0, 1)
+        dense(0, 1, 0, 1)
         o_crossing(2, 3)
+        dense(0, 1, 1, 2)
         o_mates(3)
-        o_crossing(3, 0)
+        dense(0, 1, 2)
 
     @pl.when(outer)
     def _():
@@ -1164,20 +1165,19 @@
             landed(mbuf.at[:, :, lanes], ("md",) + piece, {"tp": twin})
             both = mpart[core, :, :, lanes].astype(jnp.float32) + mbuf[:, :, lanes].astype(jnp.float32)
             msum[:, :, lanes] = both.astype(jnp.bfloat16)
+            remote(role, ("r",) + piece, lambda: (
+                msum.at[1 - chip, :, span(*piece[1:])], xrecv.at[piece[0], :, span(*piece[1:])],
+                {"sp": outward, "tp": across},
+            ), "m")
             remote(role, ("m",) + piece, lambda: (
-                msum.at[:, :, span(*piece[1:])], msum.at[:, :, span(*piece[1:])], z_out
-            ))
-
-        def relay(*piece):
-            landed(msum.at[:, :, span(*piece[1:])], ("m",) + piece, z_in)
-            remote(role, ("r",) + piece, lambda: (
-                msum.at[1 - chip, :, span(*piece[1:])], xrecv.at[piece[0], :, span(*piece[1:])], {"tp": across}
+                msum.at[chip, :, span(*piece[1:])], msum.at[chip, :, span(*piece[1:])], z_out
             ))
 
         def settle(*piece):
             j, lanes = piece[0], span(*piece[1:])
             landed(xrecv.at[j, :, lanes], ("r",) + piece, {"tp": across})
             if role == "outer" and j == 3:
+                landed(msum.at[chip, :, lanes], ("m",) + piece, z_in)
                 near = msum[chip, :, lanes].astype(jnp.float32)
             else:
                 near = part[j, core, chip, :, lanes].astype(jnp.float32) + dbuf[j, chip, :, lanes].astype(jnp.float32)
@@ -1202,18 +1202,19 @@
 
         words = {
             "emit": emit, "combine": combine, "settle": settle, "ready": ready, "pump": pump,
-            "emit_mate": emit_mate, "combine_mate": combine_mate, "relay": relay,
+            "emit_mate": emit_mate, "combine_mate": combine_mate,
         }
         for word, *piece in script:
             words[word](*piece)
 
-    opening = [("emit", 0, 0), ("emit", 0, 1), ("combine", 0, 0), ("emit", 1, 0), ("combine", 0, 1)]
+    opening = [("emit", 0, 0), ("emit", 0, 1), ("emit", 1, 0)]
     last = [(3, 1, 0, 2), (3, 1, 2, 1), (3, 1, 3, 1)]
     far = [(3, 0, 0, 2), (3, 0, 2, 2)] + last
     inner_script = (
         opening
-        + [("emit", 2, 0), ("combine", 1, 0), ("pump", 3, 1), ("ready", 2), ("emit", 2, 1), ("combine", 2, 0)]
-        + [("pump", 3, 2), ("combine", 2, 1), ("emit_mate",) + far[0], ("emit",) + far[0]]
+        + [("pump", 3, 0), ("combine", 0, 0), ("emit", 2, 0), ("combine", 0, 1), ("ready", 2), ("emit", 2, 1)]
+        + [("combine", 1, 0), ("pump", 3, 1), ("combine", 2, 0), ("combine", 2, 1), ("pump", 3, 2)]
+        + [("emit_mate",) + far[0], ("emit",) + far[0]]
         + [("pump", 3, 3), ("combine_mate",) + far[0], ("emit_mate",) + far[1], ("emit",) + far[1]]
         + [("combine",) + far[0], ("ready", 3, 0, 2), ("combine_mate",) + far[1], ("emit_mate",) + last[0]]
         + [("emit",) + last[0], ("combine",) + far[1], ("ready", 1), ("emit", 1, 1)]
@@ -1226,13 +1227,12 @@
         + [("settle",) + last[0], ("settle", 1, 1)] + [("settle",) + piece for piece in last[1:]]
     )
     outer_script = (
-        opening
-        + [("pump", 2, 1), ("ready", 1), ("emit", 1, 1), ("combine", 1, 0), ("pump", 2, 2), ("combine", 1, 1)]
-        + [("pump", 2, 3), ("emit", 2, 0), ("ready", 2, 0, 2), ("combine", 2, 0)]
-        + [("ready", 2, 2, 2), ("emit", 2, 1), ("settle", 0, 0), ("relay",) + far[0], ("combine", 2, 1)]
-        + [("settle", 0, 1), ("settle", 1, 0), ("relay",) + far[1], ("settle", 1, 1), ("relay",) + last[0]]
-        + [("settle", 2, 0), ("relay",) + last[1], ("relay",) + last[2], ("settle", 2, 1)]
-        + [("settle",) + piece for piece in far]
+        [("emit", 0, 0), ("emit", 0, 1), ("combine", 0, 0), ("emit", 1, 0), ("combine", 0, 1), ("ready", 1)]
+        + [("emit", 1, 1), ("combine", 1, 0), ("pump", 2, 1), ("combine", 1, 1), ("pump", 2, 2), ("pump", 2, 3)]
+        + [("emit", 2, 0), ("ready", 2, 0, 2), ("combine", 2, 0)]
+        + [("ready", 2, 2, 2), ("emit", 2, 1), ("settle", 0, 0), ("settle", 0, 1), ("combine", 2, 1)]
+        + [("settle", 1, 0), ("settle", 1, 1), ("settle", 2, 0), ("settle",) + far[0], ("settle", 2, 1)]
+        + [("settle",) + piece for piece in far[1:]]
     )
 
     @pl.when(inner)

time: 100 us -> 97.9 us (0.979)
  Pallas kernels: 99.3 us -> 96.9 us
    pallas_call x1, Pallas kernels: 99.3 us -> 96.9 us  [local(): pl.pallas_call(functools.partial(pair_kernel, (q_heads, kv_heads, chunks,...]
where the time goes in v5:
time: 97.9 us; the launch traced here: 97.8 us
  Pallas kernels  96.9 us (99%)
    pallas_call x1, Pallas kernels, local(): pl.pallas_call(functools.partial(pair_kernel, (q_heads, kv_heads, chunks,...  96.9 us

profile of v5, /device:TPU:0, one launch (start us, length us, event | category | flops | bytes accessed | tf_op | source)
XLA Modules:
  0.0 97.8 jit_solution(17273002383936603463)
XLA Ops:
  0.0 96.9 %shard_map.154 = bf16[96,4096]{1,0:T(8,128)(2,1)S(1)} custom-call(f32[1,4096]{1,0:T(1,128)} %bitcast.6, f32[4,128]{1,0:T(4,128)} %constant.2.clone.refs_1_, f32[1,64]{1,0:T(1,128)} %bitcast.7, f32[1,64]{1,0:T(1,128)} %bitcast.8, f32[1,64]{1,0:T(1,128)} %bitcast.9, f32[1,64]{1,0:T(1,128)} %bitcast.10, f32[1,4]{1,0:T(1,128)} %bitcast.11, ...), custom_call_target="tpu_custom_call" | custom-call | tf_op jit(solution)/shard_map/pallas_call | solution.py:1285
  96.9 0.9 copy.18

commit v6 on v5

--- a/solution.py
+++ b/solution.py
@@ -837,9 +837,9 @@
     group = q_heads // kv_heads
     pairs = q_heads // 2
 
-    def finished(k, side):
+    def finished(k, side, *tiles):
         rows = pl.ds(side * length, length)
-        for tile in range(cols // LANES):
+        for tile in tiles or range(cols // LANES):
             lanes = pl.ds(tile * LANES, LANES)
             kind = plans[k][tile * 2 * LANES // cols]
             value = proj[k % 2, rows, lanes]
@@ -1099,9 +1099,10 @@
         o_crossing(2, 0)
         twin_ready(3, 3)
         project(3, 3, (1,))
-        finished(3, 1)
+        finished(3, 1, 0)
         windowed(1, 0)
         att_outward(0)
+        finished(3, 1, 1)
         windowed(1, 1)
         att_outward(1)
         o_crossing(2, 1)

time: 97.9 us -> 98 us (level)
  no operation moved by 1% of the time
where the time goes in v6:
time: 98 us; the launch traced here: 97.9 us
  Pallas kernels  97 us (99%)
    pallas_call x1, Pallas kernels, local(): pl.pallas_call(functools.partial(pair_kernel, (q_heads, kv_heads, chunks,...  97 us

profile of v6, /device:TPU:0, one launch (start us, length us, event | category | flops | bytes accessed | tf_op | source)
XLA Modules:
  0.0 97.9 jit_solution(17066212381305675350)
XLA Ops:
  0.0 97.0 %shard_map.154 = bf16[96,4096]{1,0:T(8,128)(2,1)S(1)} custom-call(f32[1,4096]{1,0:T(1,128)} %bitcast.6, f32[4,128]{1,0:T(4,128)} %constant.2.clone.refs_1_, f32[1,64]{1,0:T(1,128)} %bitcast.7, f32[1,64]{1,0:T(1,128)} %bitcast.8, f32[1,64]{1,0:T(1,128)} %bitcast.9, f32[1,64]{1,0:T(1,128)} %bitcast.10, f32[1,4]{1,0:T(1,128)} %bitcast.11, ...), custom_call_target="tpu_custom_call" | custom-call | tf_op jit(solution)/shard_map/pallas_call | solution.py:1286
  97.0 0.9 copy.18
